TPU v7x, 1024 devices: a whole 8x8x8 slice. The times are simulated.
1024 devices in a mesh: sp: 16 (over x, core), dp: 64 (over z, y).
Axes of the slice: x: 8, y: 8, z: 8, core: 2. Of those that a mesh axis runs over, the one named last changes fastest.
Arguments:
- queries: bfloat16 [4096, 64, 512], P('sp', 'dp'), may hold values from -6 to 6
- head_keys: bfloat16 [4096, 64, 512], P('sp', 'dp'), may hold values from -6 to 6
- decay_preact: bfloat16 [4096, 64, 512], P('sp', 'dp'), may hold values from -3.2 to 3.2
- values: bfloat16 [4096, 64, 1024], P('sp', 'dp'), may hold values from -18 to 18
- extra_log_decay: float32 [256, 4096], P('dp', 'sp'), may hold values from -0.7 to 0
- decay_offset_bias: float32 [4, 128], replicated, may hold values from 0.3 to 8
- opening_state: float32 [64, 4, 128, 256], P('dp'), may hold values from -192 to 192
- output_norm_gain: float32 [256], replicated, may hold values from 0.1 to 1.9
- output_weight: bfloat16 [1024, 2048], P(None, 'dp'), may hold values from -0.1875 to 0.1875
Outputs:
- layer_out: bfloat16 [4096, 64, 2048], P('sp', 'dp')
All inputs are finite; a program needn't handle non-finite values.
Results may differ from a plain program's by a relative error of at most 0.015.
Values may be sent and summed in bfloat16 or wider, within the bound.
No kernel may reach another device: no remote copies, remote signals or barrier semaphores. Data moves between devices by JAX's collectives and lax.ppermute only.
A program may use at most 64 MiB of HBM per device.

v0:
```python
import jax
import jax.numpy as jnp
from jax import lax
from jax.sharding import PartitionSpec as P

BLOCK = 64


gate_norm_term = 16.0
norm_eps = 1e-05


def local_blocks(query_matrix, key_matrix, value_matrix, decay_logarithm):
    length, group_count, key_dim = query_matrix.shape
    value_dim = value_matrix.shape[-1]
    blocks = length // BLOCK

    def by_block(tensor):
        return tensor.reshape(blocks, BLOCK, group_count, tensor.shape[-1])

    cumulative = jnp.cumsum(by_block(decay_logarithm), axis=1)
    block_end = cumulative[:, -1]
    q_in = by_block(query_matrix) * jnp.exp(cumulative)
    k_in = by_block(key_matrix) * jnp.exp(-cumulative)
    k_out = by_block(key_matrix) * jnp.exp(block_end[:, None] - cumulative)
    block_values = by_block(value_matrix)
    causal = jnp.tril(jnp.ones((BLOCK, BLOCK), dtype=bool))
    scores = jnp.einsum("ntid,nsid->nits", q_in, k_in, precision=lax.Precision.HIGHEST)
    scores = jnp.where(causal, scores, jnp.float32(0.0))
    within = jnp.einsum("nits,nsie->ntie", scores, block_values, precision=lax.Precision.HIGHEST)
    summary = jnp.einsum("nsid,nsie->nide", k_out, block_values, precision=lax.Precision.HIGHEST)

    def advance(carried, input_arrays):
        summand, decay_end = input_arrays
        return (carried * jnp.exp(decay_end)[..., None] + summand, carried)

    empty = jnp.zeros((group_count, key_dim, value_dim), jnp.float32)
    final, starts = lax.scan(advance, empty, (summary, block_end))
    carried_out = jnp.einsum("ntid,nide->ntie", q_in, starts, precision=lax.Precision.HIGHEST)
    before = jnp.cumsum(block_end, axis=0) - block_end
    q_far = q_in * jnp.exp(before)[:, None]
    total = jnp.sum(block_end, axis=0)
    return (within + carried_out, q_far, final, total)


def on_device(
    queries,
    head_keys,
    decay_preact,
    values,
    extra_log_decay,
    decay_offset_bias,
    opening_state,
    output_norm_gain,
    output_weight,
):
    seq_tok, seqs, _ = queries.shape
    heads, key_dim = decay_offset_bias.shape
    value_dim = output_norm_gain.shape[0]
    pairs = seqs * heads
    group_size = lax.axis_size("sp")
    pair_bias = jnp.tile(decay_offset_bias, (seqs, 1))
    decay_logarithm = (
        jax.nn.log_sigmoid(
            decay_preact.astype(jnp.float32).reshape(seq_tok, pairs, key_dim) + pair_bias[None]
        )
        / gate_norm_term
        + extra_log_decay.T[:, :, None]
    )
    scaled = queries.astype(jnp.float32).reshape(seq_tok, pairs, key_dim) * key_dim ** (-0.5)
    inside, q_far, final, total = local_blocks(
        scaled,
        head_keys.astype(jnp.float32).reshape(seq_tok, pairs, key_dim),
        values.astype(jnp.float32).reshape(seq_tok, pairs, value_dim),
        decay_logarithm,
    )
    start_given = opening_state.reshape(pairs, key_dim, value_dim)
    decay_total = jnp.exp(total)
    width = value_dim // group_size
    spread_rates = jnp.broadcast_to(decay_total[None, :, :, None], (1, pairs, key_dim, group_size))
    pieces, rates = (
        lax.all_to_all(
            final[None].astype(jnp.bfloat16), "sp", split_axis=3, concat_axis=0, tiled=True
        ).astype(jnp.float32),
        lax.all_to_all(
            spread_rates.astype(jnp.bfloat16), "sp", split_axis=3, concat_axis=0, tiled=True
        ).astype(spread_rates.dtype),
    )
    own_given = lax.dynamic_slice_in_dim(start_given, lax.axis_index("sp") * width, width, 2)

    def chain(state, input_arrays):
        rate, piece = input_arrays
        return (rate * state + piece, state)

    _, starts = lax.scan(chain, own_given, (rates, pieces))
    device_start = lax.all_to_all(starts, "sp", split_axis=0, concat_axis=3, tiled=True)[0]
    from_start = jnp.einsum("ntid,ide->ntie", q_far, device_start, precision=lax.Precision.HIGHEST)
    output = (inside + from_start).reshape(seq_tok, pairs, value_dim)
    normed = (
        output
        * lax.rsqrt(jnp.mean(output * output, axis=-1, keepdims=True) + norm_eps)
        * output_norm_gain
    ).astype(jnp.bfloat16)
    token_rows = normed.reshape(seq_tok * seqs, heads * value_dim)
    result = jnp.dot(
        token_rows,
        lax.all_gather(output_weight, "dp", axis=1, tiled=True),
        preferred_element_type=jnp.float32,
    ).astype(jnp.bfloat16)
    return result.reshape(seq_tok, seqs, -1)


def solution(mesh):
    return jax.shard_map(
        on_device,
        mesh=mesh,
        in_specs=(
            P("sp", "dp", None),
            P("sp", "dp", None),
            P("sp", "dp", None),
            P("sp", "dp", None),
            P("dp", "sp"),
            P(),
            P("dp", None, None, None),
            P(),
            P(None, "dp"),
        ),
        out_specs=P("sp", "dp", None),
        check_vma=False,
    )
```

profile of v0, /device:TPU:10, one launch (start us, length us, event | category | flops | bytes accessed | tf_op | source)
XLA Modules:
  0.0 139.7 jit_solution(3105778474127985265)
XLA Ops:
  6.5 1.2 reshape.94
  7.8 0.9 copy.68
  8.6 1.5 %fusion.8 = f32[4,64,4,128]{3,2,1,0:T(4,128)S(1)} fusion(f32[4,64,4,128]{3,2,1,0:T(4,128)S(1)} %reshape.94, f32[4,64,4]{2,1,0:T(8,128)S(1)} %bitcast.96, f32[4,128]{1,0:T(4,128)} %param.18), kind=kOutput, calls=%fused_computation.23 | output fusion | flops 9699328 | bytes 1054720 | tf_op jit(solution)/shard_map/jit(cumsum)/reduce_window_sum | solution.py:21
  10.8 16.3 %all-to-all-start = ((bf16[1,4,128,16]{2,1,0,3:T(4,128)(2,1)}), bf16[1,4,128,16]{2,1,0,3:T(4,128)(2,1)S(1)}, u32[]{:S(2)}, u32[]{:S(2)}) async-start(bf16[1,4,128,16]{2,1,0,3:T(4,128)(2,1)} %broadcast_in_dim.45), calls=%async_computation | async-start | bytes 32768 | tf_op jit(solution)/shard_map/all_to_all | solution.py:85
  28.3 1.2 reshape_reshape.12
  29.5 1.5 %exponential_multiply_fusion.1 = (f32[4,64,4,128]{3,2,1,0:T(4,128)}, f32[4,64,4,128]{3,2,1,0:T(4,128)S(1)}, f32[4,64,4,128]{3,2,1,0:T(4,128)}, f32[4,64,4,128]{3,2,1,0:T(4,128)}) fusion(f32[4,64,4,128]{3,2,1,0:T(4,128)S(1)} %reshape.95, f32[4,64,4,128]{3,2,1,0:T(4,128)S(1)} %fusion.8, f32[4,4,128]{2,1,0:T(4,128)S(1)} %get-tuple-element.191, ...), kind=kLoop, calls=%fused_computation.31 | loop fusion | flops 786432 | bytes 3686400 | tf_op jit(solution)/shard_map/mul | solution.py:24
  31.0 1.0 fusion.11
  32.1 4.3 %while.26 = (s32[]{:T(128)}, f32[4,128,256]{2,1,0:T(8,128)S(1)}, f32[4,4,128,256]{3,2,1,0:T(8,128)}, f32[4,4,128]{2,1,0:T(4,128)S(1)}, f32[4,4,128,256]{3,2,1,0:T(8,128)S(1)}, /*index=5*/s32[]{:T(128)}, s32[]{:T(128)}) while((s32[]{:T(128)}, f32[4,128,256]{2,1,0:T(8,128)S(1)}, f32[4,4,128,256]{3,2,1,0:T(8,128)}, ...), condition=%wide.region_2.3_spmd.clone, body=%wide.region_1.2_spmd.clone.sunk | while | flops 524291 | bytes 2628192 | solution.py:38
  32.1 0.8 bitcast_dynamic-update-slice_fusion.5
  33.2 0.8 bitcast_dynamic-update-slice_fusion.5
  34.2 0.9 bitcast_dynamic-update-slice_fusion.5
  35.3 0.8 bitcast_dynamic-update-slice_fusion.5
  36.4 0.9 copy.76
  37.3 7.2 %all-to-all-start.1 = ((bf16[1,4,128,256]{2,1,0,3:T(4,128)(2,1)}), bf16[1,4,128,256]{2,1,0,3:T(4,128)(2,1)S(1)}, u32[]{:S(2)}, u32[]{:S(2)}) async-start(bf16[1,4,128,256]{2,1,0,3:T(4,128)(2,1)} %bitcast.13), calls=%async_computation.1 | async-start | bytes 524288 | tf_op jit(solution)/shard_map/all_to_all | solution.py:82
  44.9 7.9 %all-to-all-done.1 = bf16[1,4,128,256]{2,1,0,3:T(4,128)(2,1)S(1)} async-done(((bf16[1,4,128,256]{2,1,0,3:T(4,128)(2,1)}), bf16[1,4,128,256]{2,1,0,3:T(4,128)(2,1)S(1)}, u32[]{:S(2)}, u32[]{:S(2)}) %all-to-all-start.1) | async-done | bytes 262176 | tf_op jit(solution)/shard_map/all_to_all | solution.py:82
  52.9 10.3 %while.25 = (s32[]{:T(128)}, f32[4,128,16]{1,2,0:T(8,128)S(1)}, f32[16,4,128,16]{2,3,1,0:T(8,128)}, f32[16,4,128,1]{2,1,3,0:T(4,128)S(1)}, f32[16,4,128,16]{2,3,0,1:T(8,128)S(1)}, /*index=5*/s32[]{:T(128)}) while((s32[]{:T(128)}, f32[4,128,16]{1,2,0:T(8,128)S(1)}, f32[16,4,128,16]{2,3,1,0:T(8,128)}, f32[16,4,128,1]{2,1,3,0:T(4,128)S(1)}, ...), condition=%wide.region_5.6_spmd, body=%wide.region_4.5_spmd.sunk | while | flops 16386 | bytes 170573 | solution.py:95
  63.2 7.0 %all-to-all-start.2 = ((f32[16,4,128,16]{2,3,1,0:T(8,128)}), f32[16,4,128,16]{2,3,1,0:T(8,128)}, u32[]{:S(2)}, u32[]{:S(2)}) async-start(f32[16,4,128,16]{2,3,1,0:T(8,128)} %get-tuple-element.62), calls=%async_computation.2 | async-start | bytes 1048576 | tf_op jit(solution)/shard_map/all_to_all | solution.py:96
  70.3 1.0 convolution_select_fusion
  71.3 3.0 %convolution_bitcast_fusion = f32[4,64,4,256]{3,1,2,0:T(8,128)S(1)} fusion(f32[4,4,128,256]{3,2,1,0:T(8,128)} %get-tuple-element.60, f32[4,64,4,128]{3,2,1,0:T(4,128)S(1)} %copy-done.1), kind=kOutput, calls=%fused_computation.9 | convolution fusion | flops 402653184 | bytes 3670016 | tf_op jit(solution)/shard_map/ntid,nide->ntie/dot_general | solution.py:39
  74.9 9.3 %all-to-all-done.2 = f32[16,4,128,16]{2,3,1,0:T(8,128)} async-done(((f32[16,4,128,16]{2,3,1,0:T(8,128)}), f32[16,4,128,16]{2,3,1,0:T(8,128)}, u32[]{:S(2)}, u32[]{:S(2)}) %all-to-all-start.2) | async-done | bytes 524320 | tf_op jit(solution)/shard_map/all_to_all | solution.py:96
  84.2 1.1 copy.61
  85.3 1.1 multiply_reduce_fusion
  88.0 40.4 %all-gather.2.cloned.1.call-done = bf16[1024,2048]{0,1:T(8,128)(2,1)} async-done(((bf16[1024,32]{0,1:T(8,128)(2,1)}), bf16[1024,2048]{0,1:T(8,128)(2,1)}) %all-gather.2.cloned.1.call-update) | async-done | bytes 4194320 | tf_op jit(solution)/shard_map/all_gather | solution.py:107
  128.4 4.5 %fusion = bf16[256,1,2048]{2,0,1:T(8,128)(2,1)} fusion(bf16[1024,2048]{0,1:T(8,128)(2,1)} %all-gather.2.cloned.1.call-done, f32[256,1024]{1,0:T(8,128)S(1)} %bitcast.92, f32[256,1024]{1,0:T(8,128)S(1)} %bitcast.91, f32[1024]{0:T(1024)S(1)} %bitcast.98), kind=kOutput, calls=%fused_computation.7 | convolution fusion | flops 1075052544 | bytes 7344128 | tf_op jit(solution)/shard_map/dot_general | solution.py:105
  (105 shorter events, 15.2 us)
Async XLA Ops:
  6.5 38.0 %copy-start = (f32[1,4,128,256]{3,2,1,0:T(8,128)S(1)}, f32[1,4,128,256]{3,2,1,0:T(8,128)}, u32[]{:S(2)}) copy-start(f32[1,4,128,256]{3,2,1,0:T(8,128)} %param.19) | copy-start | bytes 1572868
  6.5 21.3 %copy-start.7 = (bf16[256,1,512]{2,0,1:T(8,128)(2,1)S(1)}, bf16[256,1,512]{2,0,1:T(8,128)(2,1)}, u32[]{:S(2)}) copy-start(bf16[256,1,512]{2,0,1:T(8,128)(2,1)} %param.13) | copy-start | bytes 786436
  6.5 21.6 %copy-start.8 = (bf16[256,1,512]{2,0,1:T(8,128)(2,1)S(1)}, bf16[256,1,512]{2,0,1:T(8,128)(2,1)}, u32[]{:S(2)}) copy-start(bf16[256,1,512]{2,0,1:T(8,128)(2,1)} %param.14) | copy-start | bytes 786436
  7.7 20.6 %copy-start.6 = (bf16[256,1,1024]{2,0,1:T(8,128)(2,1)S(1)}, bf16[256,1,1024]{2,0,1:T(8,128)(2,1)}, u32[]{:S(2)}) copy-start(bf16[256,1,1024]{2,0,1:T(8,128)(2,1)} %param.16) | copy-start | bytes 1572868
  10.8 26.6 %all-to-all-start = ((bf16[1,4,128,16]{2,1,0,3:T(4,128)(2,1)}), bf16[1,4,128,16]{2,1,0,3:T(4,128)(2,1)S(1)}, u32[]{:S(2)}, u32[]{:S(2)}) async-start(bf16[1,4,128,16]{2,1,0,3:T(4,128)(2,1)} %broadcast_in_dim.45), calls=%async_computation | async-start | bytes 32768 | tf_op jit(solution)/shard_map/all_to_all | solution.py:85
  27.1 101.3 %all-gather.2.cloned.1.call-start = ((), (), s32[]{:S(2)}) async-start(), calls=%async_computation.3 | async-start | bytes 4259840 | tf_op jit(solution)/shard_map/all_gather | solution.py:107
  29.5 1.5 %copy-start.2 = (bf16[4,64,4,256]{3,2,1,0:T(4,128)(2,1)S(1)}, bf16[4,64,4,256]{3,2,1,0:T(4,128)(2,1)}, u32[]{:S(2)}) copy-start(bf16[4,64,4,256]{3,2,1,0:T(4,128)(2,1)} %reshape_reshape.12) | copy-start | bytes 1572868
  36.4 8.4 %copy-start.9 = (f32[256]{0:T(256)S(1)}, f32[256]{0:T(256)}, u32[]{:S(2)}) copy-start(f32[256]{0:T(256)} %param.20) | copy-start | bytes 3076
  37.3 15.5 %all-to-all-start.1 = ((bf16[1,4,128,256]{2,1,0,3:T(4,128)(2,1)}), bf16[1,4,128,256]{2,1,0,3:T(4,128)(2,1)S(1)}, u32[]{:S(2)}, u32[]{:S(2)}) async-start(bf16[1,4,128,256]{2,1,0,3:T(4,128)(2,1)} %bitcast.13), calls=%async_computation.1 | async-start | bytes 524288 | tf_op jit(solution)/shard_map/all_to_all | solution.py:82
  44.6 25.7 %copy-start.1 = (f32[4,64,4,128]{3,2,1,0:T(4,128)S(1)}, f32[4,64,4,128]{3,2,1,0:T(4,128)}, u32[]{:S(2)}) copy-start(f32[4,64,4,128]{3,2,1,0:T(4,128)} %get-tuple-element.123) | copy-start | bytes 1572868
  44.6 25.7 %copy-start.4 = (f32[4,64,4,128]{3,2,1,0:T(4,128)S(1)}, f32[4,64,4,128]{3,2,1,0:T(4,128)}, u32[]{:S(2)}) copy-start(f32[4,64,4,128]{3,2,1,0:T(4,128)} %get-tuple-element.118) | copy-start | bytes 1572868
  63.2 21.0 %all-to-all-start.2 = ((f32[16,4,128,16]{2,3,1,0:T(8,128)}), f32[16,4,128,16]{2,3,1,0:T(8,128)}, u32[]{:S(2)}, u32[]{:S(2)}) async-start(f32[16,4,128,16]{2,3,1,0:T(8,128)} %get-tuple-element.62), calls=%async_computation.2 | async-start | bytes 1048576 | tf_op jit(solution)/shard_map/all_to_all | solution.py:96
  71.3 3.0 %copy-start.3 = (bf16[4,64,4,256]{3,2,1,0:T(4,128)(2,1)S(1)}, bf16[4,64,4,256]{3,2,1,0:T(4,128)(2,1)}, u32[]{:S(2)}) copy-start(bf16[4,64,4,256]{3,2,1,0:T(4,128)(2,1)} %reshape_reshape.12) | copy-start | bytes 1572868
  74.3 11.0 %copy-start.5 = (f32[4,64,4,128]{3,2,1,0:T(4,128)S(1)}, f32[4,64,4,128]{3,2,1,0:T(4,128)}, u32[]{:S(2)}) copy-start(f32[4,64,4,128]{3,2,1,0:T(4,128)} %get-tuple-element.122) | copy-start | bytes 1572868
Sparse Core Ops, SparseCore 0:
  32.1 96.2 all-gather.1
where the time goes:
time: 140 us
  waiting for transfers between devices  58.3 us (42%)
  starting transfers between devices  30.6 us (22%)
  local copies, waits for them, and re-layouts  18 us (13%)
  between operations  13.7 us (10%)
  matrix products  11.2 us (8%)
  other arithmetic  7.55 us (5%)
    all_gather x1, waiting for transfers between devices, on_device(): lax.all_gather(output_weight, 'dp', axis=1, tiled=True)  40.4 us
    all_to_all x1, starting transfers between devices, on_device(): lax.all_to_all(spread_rates.astype(jnp.bfloat16), 'sp', split_axis=3, con...  16.3 us
    dynamic_update_slice x16, local copies, waits for them, and re-layouts, on_device(): _, starts = lax.scan(chain, own_given, (rates, pieces))  9.89 us
    all_to_all x1, waiting for transfers between devices, on_device(): lax.all_to_all(starts, 'sp', split_axis=0, concat_axis=3, tiled=True)[0]  9.3 us
    all_to_all x1, waiting for transfers between devices, on_device(): lax.all_to_all(final[None].astype(jnp.bfloat16), 'sp', split_axis=3, conc...  7.93 us
    all_to_all x1, starting transfers between devices, on_device(): lax.all_to_all(final[None].astype(jnp.bfloat16), 'sp', split_axis=3, conc...  7.21 us
    all_to_all x1, starting transfers between devices, on_device(): lax.all_to_all(starts, 'sp', split_axis=0, concat_axis=3, tiled=True)[0]  7.04 us
    dot_general x1, matrix products, on_device(): jnp.dot(token_rows, lax.all_gather(output_weight, 'dp', axis=1, tiled=Tru...  4.45 us
  transfers between devices with their start and end apart: 4, of which 3 were waited for; matrix products, arithmetic and copies ran while one was open for 20% of the time, Pallas kernels for 0%

commit v1 on v0

v1 whole, which is shorter than its diff:
```python
import jax
import jax.numpy as jnp
from jax import lax
from jax.experimental import pallas as pl
from jax.experimental.pallas import tpu as pltpu
from jax.sharding import PartitionSpec as P

BLOCK = 64
gate_norm_term = 16.0
norm_eps = 1e-05
F32 = jnp.float32
BF16 = jnp.bfloat16
VMEM = pl.BlockSpec(memory_space=pltpu.VMEM)


def dot(a, b, dims=(((1,), (0,)), ((), ()))):
    return lax.dot_general(a, b, dims, preferred_element_type=F32)


NT = (((1,), (1,)), ((), ()))
TN = (((0,), (0,)), ((), ()))


def summary_kernel(k_ref, x_ref, v_ref, extra_ref, bias_ref, send_ref, cum_ref):
    tok = k_ref.shape[0]
    heads, kd = bias_ref.shape
    vd = v_ref.shape[1] // heads
    per, rows = send_ref.shape[0] // heads, kd * heads // send_ref.shape[0]
    spikes = jnp.transpose(extra_ref[...])
    tri = (
        lax.broadcasted_iota(jnp.int32, (tok, tok), 0)
        >= lax.broadcasted_iota(jnp.int32, (tok, tok), 1)
    ).astype(BF16)
    for h in range(heads):
        cols = slice(h * kd, (h + 1) * kd)
        x = x_ref[:, cols].astype(F32) + bias_ref[h : h + 1, :]
        log_sig = jnp.minimum(x, 0.0) - jnp.log(1.0 + jnp.exp(-jnp.abs(x)))
        decay = log_sig * (1.0 / gate_norm_term) + spikes[:, h : h + 1]
        high = decay.astype(BF16)
        rest = decay - high.astype(F32)
        mid = rest.astype(BF16)
        low = (rest - mid.astype(F32)).astype(BF16)
        cum = dot(tri, high) + dot(tri, mid) + dot(tri, low)
        cum_ref[:, cols] = cum
        total = cum[tok - 1 : tok, :]
        k_out = (k_ref[:, cols].astype(F32) * jnp.exp(total - cum)).astype(BF16)
        final = dot(k_out, v_ref[:, h * vd : (h + 1) * vd], TN).astype(BF16)
        rate = jnp.broadcast_to(jnp.exp(total), (8, kd))
        for r in range(per):
            send_ref[h * per + r, 0:rows, :] = final[r * rows : (r + 1) * rows, :]
            turned = pltpu.roll(rate, (kd - r * rows) % kd, 1) if r else rate
            coarse = turned.astype(BF16)
            fine = (turned - coarse.astype(F32)).astype(BF16)
            send_ref[h * per + r, rows : rows + 8, :] = jnp.concatenate([coarse, fine], axis=1)


def inside_kernel(q_ref, k_ref, v_ref, cum_ref, inside_ref, far_ref):
    tok, width = q_ref.shape
    kd = 128
    heads = width // kd
    vd = v_ref.shape[1] // heads
    scale = kd ** (-0.5)
    for h in range(heads):
        cols = slice(h * kd, (h + 1) * kd)
        vcols = slice(h * vd, (h + 1) * vd)
        for i in range(tok // BLOCK):
            lo, hi = i * BLOCK, (i + 1) * BLOCK
            q = q_ref[lo:hi, cols].astype(F32) * scale
            cum = cum_ref[lo:hi, cols]
            far_ref[lo:hi, cols] = (q * jnp.exp(cum)).astype(BF16)
            if i:
                base = cum_ref[lo - 1 : lo, cols]
                q_in = (q * jnp.exp(cum - base)).astype(BF16)
                k_in = (k_ref[0:hi, cols].astype(F32) * jnp.exp(base - cum_ref[0:hi, cols])).astype(BF16)
            else:
                q_in = (q * jnp.exp(cum)).astype(BF16)
                k_in = (k_ref[0:hi, cols].astype(F32) * jnp.exp(-cum)).astype(BF16)
            scores = dot(q_in, k_in, NT)
            seen = (
                lax.broadcasted_iota(jnp.int32, (BLOCK, hi), 0) + lo
                >= lax.broadcasted_iota(jnp.int32, (BLOCK, hi), 1)
            )
            scores = jnp.where(seen, scores, 0.0).astype(BF16)
            inside_ref[lo:hi, vcols] = dot(scores, v_ref[0:hi, vcols])


def chain_kernel(who_ref, got_ref, open_ref, out_ref):
    group = got_ref.shape[0]
    rows = out_ref.shape[1]
    state = open_ref[...]
    where = lax.broadcasted_iota(jnp.int32, (8, 128), 0)
    parts = []
    for g in range(group // 8):
        table = jnp.zeros((8, 128), F32)
        for d in range(8):
            pair = got_ref[g * 8 + d, rows : rows + 8, :].astype(F32)
            table = jnp.where(where == d, pair[:, 0:128] + pair[:, 128:256], table)
        parts.append(table)
    rates = jnp.transpose(jnp.concatenate(parts, axis=0))
    for d in range(group):
        out_ref[d] = state.astype(BF16)
        if d < group - 1:
            state = rates[0:rows, d : d + 1] * state + got_ref[d, 0:rows, :].astype(F32)


def project_kernel(who_ref, inside_ref, far_ref, start_ref, gain_ref, mine_ref, other_ref, out_ref, normed):
    heads = 4
    kd, vd = far_ref.shape[1] // heads, start_ref.shape[1]
    half = mine_ref.shape[1]

    @pl.when(pl.program_id(0) == 0)
    def _():
        for h in range(heads):
            o = inside_ref[:, h * vd : (h + 1) * vd] + dot(
                far_ref[:, h * kd : (h + 1) * kd], start_ref[h * kd : (h + 1) * kd, :]
            )
            spread = lax.rsqrt(jnp.mean(o * o, axis=-1, keepdims=True) + norm_eps)
            normed[:, h * vd : (h + 1) * vd] = (o * spread * gain_ref[...]).astype(BF16)

    core = who_ref[1]
    first = normed[:, pl.ds(pl.multiple_of(core * half, half), half)]
    second = normed[:, pl.ds(pl.multiple_of((1 - core) * half, half), half)]
    out_ref[...] = (dot(first, mine_ref[...], NT) + dot(second, other_ref[...], NT)).astype(BF16)


def on_device(
    queries,
    head_keys,
    decay_preact,
    values,
    extra_log_decay,
    decay_offset_bias,
    opening_state,
    output_norm_gain,
    output_weight,
):
    tok, seqs, width = queries.shape
    heads, kd = decay_offset_bias.shape
    vd = output_norm_gain.shape[0]
    group = lax.axis_size("sp")
    columns_group = lax.axis_size("dp")
    share = output_weight.shape[1]
    model = share * columns_group
    rows = heads * kd // group
    sp = lax.axis_index("sp")
    core = lax.rem(sp, 2)
    who = jnp.stack([sp, core]).astype(jnp.int32)
    half = heads * vd // 2

    q = queries.reshape(tok, width)
    k = head_keys.reshape(tok, width)
    x = decay_preact.reshape(tok, width)
    v = values.reshape(tok, heads * vd)
    opening = opening_state.reshape(heads * kd, vd)

    part = lax.dynamic_slice_in_dim(output_weight.T, core * half, half, 1)
    spread_part = jnp.broadcast_to(part[None], (columns_group, share, half))
    mine = lax.all_to_all(spread_part, "dp", 0, 0, tiled=True).reshape(model, half)
    other = lax.ppermute(mine, "sp", [(i, i ^ 1) for i in range(group)])

    send, cum = pl.pallas_call(
        summary_kernel,
        out_shape=(
            jax.ShapeDtypeStruct((group, rows + 8, vd), BF16),
            jax.ShapeDtypeStruct((tok, width), F32),
        ),
        in_specs=[VMEM] * 5,
        out_specs=(VMEM, VMEM),
        cost_estimate=pl.CostEstimate(flops=10**9, bytes_accessed=2 * 10**6, transcendentals=10**6),
        name="summary",
    )(k, x, v, extra_log_decay, decay_offset_bias)

    got = lax.all_to_all(send, "sp", 0, 0, tiled=True)

    inside, far = pl.pallas_call(
        inside_kernel,
        out_shape=(
            jax.ShapeDtypeStruct((tok, heads * vd), F32),
            jax.ShapeDtypeStruct((tok, width), BF16),
        ),
        in_specs=[VMEM] * 4,
        out_specs=(VMEM, VMEM),
        cost_estimate=pl.CostEstimate(flops=3 * 10**9, bytes_accessed=3 * 10**6, transcendentals=10**6),
        name="inside",
    )(q, k, v, cum)

    starts = pl.pallas_call(
        chain_kernel,
        out_shape=jax.ShapeDtypeStruct((group, rows, vd), BF16),
        grid_spec=pltpu.PrefetchScalarGridSpec(
            num_scalar_prefetch=1,
            grid=(1,),
            in_specs=[
                pl.BlockSpec((group, rows + 8, vd), lambda i, who: (0, 0, 0)),
                pl.BlockSpec((rows, vd), lambda i, who: (who[0], 0)),
            ],
            out_specs=pl.BlockSpec((group, rows, vd), lambda i, who: (0, 0, 0)),
        ),
        name="chain",
    )(who, got, opening)

    start = lax.all_to_all(starts, "sp", 0, 0, tiled=True).reshape(heads * kd, vd)

    tile = 512
    out = pl.pallas_call(
        project_kernel,
        out_shape=jax.ShapeDtypeStruct((tok, model), BF16),
        grid_spec=pltpu.PrefetchScalarGridSpec(
            num_scalar_prefetch=1,
            grid=(model // tile,),
            in_specs=[
                pl.BlockSpec((tok, heads * vd), lambda i, who: (0, 0)),
                pl.BlockSpec((tok, width), lambda i, who: (0, 0)),
                pl.BlockSpec((heads * kd, vd), lambda i, who: (0, 0)),
                pl.BlockSpec((1, vd), lambda i, who: (0, 0)),
                pl.BlockSpec((tile, half), lambda i, who: (i, 0)),
                pl.BlockSpec((tile, half), lambda i, who: (i, 0)),
            ],
            out_specs=pl.BlockSpec((tok, tile), lambda i, who: (0, i)),
            scratch_shapes=[pltpu.VMEM((tok, heads * vd), BF16)],
        ),
        name="project",
    )(who, inside, far, start, output_norm_gain.reshape(1, vd), mine, other)
    return out.reshape(tok, seqs, model)


def solution(mesh):
    return jax.shard_map(
        on_device,
        mesh=mesh,
        in_specs=(
            P("sp", "dp", None),
            P("sp", "dp", None),
            P("sp", "dp", None),
            P("sp", "dp", None),
            P("dp", "sp"),
            P(),
            P("dp", None, None, None),
            P(),
            P(None, "dp"),
        ),
        out_specs=P("sp", "dp", None),
        check_vma=False,
    )
```

time: 140 us -> 129 us (0.921)
  the two profiles are of different devices: /device:TPU:10 before, /device:TPU:1 now
where the time goes in v1:
time: 129 us
  blocking collectives  73 us (57%)
  waiting for transfers between devices  19.1 us (15%)
  Pallas kernels  17.2 us (13%)
  starting transfers between devices  16.1 us (12%)
  local copies, waits for them, and re-layouts  2.53 us (2%)
    all_to_all x1, blocking collectives, on_device(): lax.all_to_all(spread_part, 'dp', 0, 0, tiled=True).reshape(model, half)  73 us
    all_to_all x1, waiting for transfers between devices, on_device(): got = lax.all_to_all(send, 'sp', 0, 0, tiled=True)  12.4 us
    all_to_all x1, starting transfers between devices, on_device(): got = lax.all_to_all(send, 'sp', 0, 0, tiled=True)  6.89 us
    all_to_all x1, waiting for transfers between devices, on_device(): lax.all_to_all(starts, 'sp', 0, 0, tiled=True).reshape(heads * kd, vd)  6.75 us
    pallas_call x1, Pallas kernels, on_device(): pl.pallas_call(project_kernel, out_shape=jax.ShapeDtypeStruct((tok, model...  6.38 us
    ppermute x1, starting transfers between devices, on_device(): other = lax.ppermute(mine, 'sp', [(i, i ^ 1) for i in range(group)])  5.76 us
    pallas_call x1, Pallas kernels, on_device(): pl.pallas_call(inside_kernel, out_shape=(jax.ShapeDtypeStruct((tok, heads...  4.37 us
    pallas_call x1, Pallas kernels, on_device(): pl.pallas_call(summary_kernel, out_shape=(jax.ShapeDtypeStruct((group, ro...  3.89 us
  transfers between devices with their start and end apart: 3, of which 2 were waited for; matrix products, arithmetic and copies ran while one was open for 0% of the time, Pallas kernels for 8%

profile of v1, /device:TPU:1, one launch (start us, length us, event | category | flops | bytes accessed | tf_op | source)
XLA Modules:
  0.0 128.6 jit_solution(17772093437447462625)
XLA Ops:
  0.0 0.0 copy-start
  0.0 0.8 copy-done
  0.8 0.2 broadcast_in_dim.2
  1.1 73.0 %all_to_all.15 = bf16[64,32,512]{2,1,0:T(8,128)(2,1)S(1)} all-to-all(bf16[64,32,512]{2,1,0:T(8,128)(2,1)S(1)} %broadcast_in_dim.2), channel_id=1, replica_groups=mesh['sp'=16,'dp'=64] {'dp'}, dimensions={0} | all-to-all | bytes 4194304 | tf_op jit(solution)/shard_map/all_to_all | solution.py:158
  74.1 0.0 copy-start.1
  74.1 5.8 %collective-permute-start = (bf16[2048,512]{1,0:T(8,128)(2,1)S(1)}, bf16[2048,512]{1,0:T(8,128)(2,1)}, u32[]{:S(2)}, u32[]{:S(2)}) collective-permute-start(bf16[2048,512]{1,0:T(8,128)(2,1)S(1)} %bitcast.13), channel_id=1, source_target_pairs={{0,64},{64,0},{128,192},{192,128},{256,320},{320,256},{384,448},{4... | collective-permute-start | bytes 6291464 | tf_op jit(solution)/shard_map/ppermute | solution.py:159
  79.9 3.9 %summary.1 = (bf16[16,40,256]{2,1,0:T(8,128)(2,1)}, f32[256,512]{1,0:T(8,128)}) custom-call(bf16[256,512]{1,0:T(8,128)(2,1)} %bitcast.22, bf16[256,512]{1,0:T(8,128)(2,1)} %bitcast.20, bf16[256,1024]{1,0:T(8,128)(2,1)} %bitcast.18, f32[4,256]{1,0:T(4,128)} %extra_ref.1, f32[4,128]{1,0:T(4,128)} %bias_ref.1), custom_call_target="tpu_custom_call" | custom-call | flops 1000000000 | bytes 2000000 | tf_op jit(solution)/shard_map/summary/pallas_call | solution.py:161
  83.8 0.0 copy-done.1
  83.8 6.9 %all-to-all-start = ((bf16[16,40,256]{2,1,0:T(8,128)(2,1)}), bf16[16,40,256]{2,1,0:T(8,128)(2,1)S(1)}, u32[]{:S(2)}, u32[]{:S(2)}) async-start(bf16[16,40,256]{2,1,0:T(8,128)(2,1)} %get-tuple-element.12), calls=%async_computation | async-start | bytes 655360 | tf_op jit(solution)/shard_map/all_to_all | solution.py:173
  90.7 0.6 pad_add_fusion.who_ref
  91.3 12.4 %all-to-all-done.got_ref = bf16[16,40,256]{2,1,0:T(8,128)(2,1)S(1)} async-done(((bf16[16,40,256]{2,1,0:T(8,128)(2,1)}), bf16[16,40,256]{2,1,0:T(8,128)(2,1)S(1)}, u32[]{:S(2)}, u32[]{:S(2)}) %all-to-all-start) | async-done | bytes 327712 | tf_op jit(solution)/shard_map/all_to_all | solution.py:173
  103.7 0.0 copy-start.2
  103.7 0.7 copy-done.2
  104.4 2.6 %chain.1 = bf16[16,32,256]{2,1,0:T(8,128)(2,1)} custom-call(s32[2]{0:T(128)} %pad_add_fusion.who_ref, bf16[16,40,256]{2,1,0:T(8,128)(2,1)} %copy-done.2, f32[512,256]{1,0:T(8,128)} %bitcast.16), custom_call_target="tpu_custom_call" | custom-call | tf_op jit(solution)/shard_map/chain/pallas_call | solution.py:187
  107.0 3.4 %all-to-all-start.1 = ((bf16[16,32,256]{2,1,0:T(8,128)(2,1)}), bf16[16,32,256]{2,1,0:T(8,128)(2,1)S(1)}, u32[]{:S(2)}, u32[]{:S(2)}) async-start(bf16[16,32,256]{2,1,0:T(8,128)(2,1)} %chain.1), calls=%async_computation.1 | async-start | bytes 524288 | tf_op jit(solution)/shard_map/all_to_all | solution.py:202
  110.4 4.4 %inside.1 = (f32[256,1024]{1,0:T(8,128)}, bf16[256,512]{1,0:T(8,128)(2,1)}) custom-call(bf16[256,512]{1,0:T(8,128)(2,1)} %bitcast.21, bf16[256,512]{1,0:T(8,128)(2,1)} %bitcast.23, bf16[256,1024]{1,0:T(8,128)(2,1)} %bitcast.19, f32[256,512]{1,0:T(8,128)} %get-tuple-element.9.cum_ref), custom_call_target="tpu_custom_call" | custom-call | flops 3000000000 | bytes 3000000 | tf_op jit(solution)/shard_map/inside/pallas_call | solution.py:175
  114.8 6.8 %all-to-all-done.1 = bf16[16,32,256]{2,1,0:T(8,128)(2,1)S(1)} async-done(((bf16[16,32,256]{2,1,0:T(8,128)(2,1)}), bf16[16,32,256]{2,1,0:T(8,128)(2,1)S(1)}, u32[]{:S(2)}, u32[]{:S(2)}) %all-to-all-start.1) | async-done | bytes 262176 | tf_op jit(solution)/shard_map/all_to_all | solution.py:202
  121.5 0.0 copy-start.3
  121.5 0.0 collective-permute-done.other_ref
  121.5 0.7 copy-done.3
  122.3 6.4 %project.1 = bf16[256,2048]{1,0:T(8,128)(2,1)} custom-call(s32[2]{0:T(128)} %pad_add_fusion.who_ref, f32[256,1024]{1,0:T(8,128)} %get-tuple-element.10.inside_ref, bf16[256,512]{1,0:T(8,128)(2,1)} %get-tuple-element.11.far_ref, bf16[512,256]{1,0:T(8,128)(2,1)} %bitcast.15, f32[1,256]{1,0:T(1,128)} %bitcast.17, bf16[2048,512]{1,0:T(8,128)(2,1)} %bitcast.14, ...), custom_call_target="tpu_custom_call" | custom-call | tf_op jit(solution)/shard_map/project/pallas_call | solution.py:205
  (1 shorter events, 0.0 us)
Async XLA Ops:
  0.0 0.8 copy-start
  74.1 9.7 %copy-start.1 = (bf16[64,32,512]{2,1,0:T(8,128)(2,1)}, bf16[64,32,512]{2,1,0:T(8,128)(2,1)S(1)}, u32[]{:S(2)}) copy-start(bf16[64,32,512]{2,1,0:T(8,128)(2,1)S(1)} %all_to_all.15) | copy-start | bytes 6291460
  74.1 47.4 %collective-permute-start = (bf16[2048,512]{1,0:T(8,128)(2,1)S(1)}, bf16[2048,512]{1,0:T(8,128)(2,1)}, u32[]{:S(2)}, u32[]{:S(2)}) collective-permute-start(bf16[2048,512]{1,0:T(8,128)(2,1)S(1)} %bitcast.13), channel_id=1, source_target_pairs={{0,64},{64,0},{128,192},{192,128},{256,320},{320,256},{384,448},{4... | collective-permute-start | bytes 6291464 | tf_op jit(solution)/shard_map/ppermute | solution.py:159
  83.8 19.9 %all-to-all-start = ((bf16[16,40,256]{2,1,0:T(8,128)(2,1)}), bf16[16,40,256]{2,1,0:T(8,128)(2,1)S(1)}, u32[]{:S(2)}, u32[]{:S(2)}) async-start(bf16[16,40,256]{2,1,0:T(8,128)(2,1)} %get-tuple-element.12), calls=%async_computation | async-start | bytes 655360 | tf_op jit(solution)/shard_map/all_to_all | solution.py:173
  103.7 0.7 copy-start.2
  107.0 14.6 %all-to-all-start.1 = ((bf16[16,32,256]{2,1,0:T(8,128)(2,1)}), bf16[16,32,256]{2,1,0:T(8,128)(2,1)S(1)}, u32[]{:S(2)}, u32[]{:S(2)}) async-start(bf16[16,32,256]{2,1,0:T(8,128)(2,1)} %chain.1), calls=%async_computation.1 | async-start | bytes 524288 | tf_op jit(solution)/shard_map/all_to_all | solution.py:202
  121.5 0.7 copy-start.3

commit v2 on v1

v2 whole, which is shorter than its diff:
```python
import jax
import jax.numpy as jnp
from jax import lax
from jax.experimental import pallas as pl
from jax.experimental.pallas import tpu as pltpu
from jax.sharding import PartitionSpec as P


BLOCK = 64
gate_norm_term = 16.0
norm_eps = 1e-05
F32 = jnp.float32
BF16 = jnp.bfloat16
VMEM = pl.BlockSpec(memory_space=pltpu.VMEM)
HBM = pl.BlockSpec(memory_space=pltpu.HBM)
SMEM = pl.BlockSpec(memory_space=pltpu.SMEM)
SIDE = 8
TILES = 4


def dot(a, b, dims=(((1,), (0,)), ((), ()))):
    return lax.dot_general(a, b, dims, preferred_element_type=F32)


NT = (((1,), (1,)), ((), ()))
TN = (((0,), (0,)), ((), ()))


def fetch(sems, *pairs):
    copies = [pltpu.make_async_copy(a, b, sems.at[n]) for n, (a, b) in enumerate(pairs)]
    for c in copies:
        c.start()
    return copies


def spread_kernel(who_ref, weight_hbm, out_ref, quarters, sems):
    core = who_ref[1]
    width = out_ref.shape[2]
    pairs = []
    for c in range(4):
        first = pl.multiple_of((core * 4 + c) * width, width)
        pairs.append((weight_hbm.at[:, pl.ds(first, width)], quarters.at[c]))
    for c in fetch(sems, *pairs):
        c.wait()
    for d in range(out_ref.shape[0]):
        out_ref[d] = quarters[(d % SIDE + 2 * (d // SIDE)) % 4]


def summary_kernel(k_hbm, x_hbm, v_hbm, extra_hbm, bias_hbm, send_ref, cum_ref, k_ref, x_ref, v_ref, extra_ref, bias_ref, sems):
    get_x, get_extra, get_bias, get_k, get_v = fetch(
        sems, (x_hbm, x_ref), (extra_hbm, extra_ref), (bias_hbm, bias_ref), (k_hbm, k_ref), (v_hbm, v_ref)
    )
    tok = k_ref.shape[0]
    heads, kd = bias_ref.shape
    vd = v_ref.shape[1] // heads
    per, rows = send_ref.shape[0] // heads, kd * heads // send_ref.shape[0]
    wide = vd // kd
    tri = (
        lax.broadcasted_iota(jnp.int32, (tok, tok), 0)
        >= lax.broadcasted_iota(jnp.int32, (tok, tok), 1)
    ).astype(BF16)
    odd = lax.broadcasted_iota(jnp.int32, (8, kd), 0) % 2 == 1
    get_extra.wait()
    spikes = jnp.transpose(extra_ref[...])
    get_bias.wait()
    get_x.wait()
    for h in range(heads):
        cols = slice(h * kd, (h + 1) * kd)
        x = x_ref[:, cols].astype(F32) + bias_ref[h : h + 1, :]
        log_sig = jnp.minimum(x, 0.0) - jnp.log(1.0 + jnp.exp(-jnp.abs(x)))
        decay = log_sig * (1.0 / gate_norm_term) + spikes[:, h : h + 1]
        high = decay.astype(BF16)
        rest = decay - high.astype(F32)
        mid = rest.astype(BF16)
        low = (rest - mid.astype(F32)).astype(BF16)
        cum = dot(tri, high) + dot(tri, mid) + dot(tri, low)
        cum_ref[:, cols] = cum
        total = cum[tok - 1 : tok, :]
        if h == 0:
            get_k.wait()
            get_v.wait()
        k_out = (k_ref[:, cols].astype(F32) * jnp.exp(total - cum)).astype(BF16)
        final = dot(k_out, v_ref[:, h * vd : (h + 1) * vd], TN).astype(BF16)
        rate = jnp.broadcast_to(jnp.exp(total), (8, kd))
        for r in range(per):
            for w in range(wide):
                send_ref[h * per + r, w * rows : (w + 1) * rows, :] = final[
                    r * rows : (r + 1) * rows, w * kd : (w + 1) * kd
                ]
            turned = pltpu.roll(rate, (kd - r * rows) % kd, 1) if r else rate
            coarse = turned.astype(BF16).astype(F32)
            send_ref[h * per + r, wide * rows : wide * rows + 8, :] = jnp.where(
                odd, turned - coarse, coarse
            ).astype(BF16)


def inside_kernel(
    who_ref, cum_ref, q_hbm, k_hbm, v_hbm, open_hbm, inside_ref, far_ref, open_ref, q_ref, k_ref, v_ref, sems
):
    mine = open_ref.shape[0]
    first = pl.multiple_of(who_ref[0] * mine, mine)
    for c in fetch(
        sems, (q_hbm, q_ref), (k_hbm, k_ref), (v_hbm, v_ref), (open_hbm.at[pl.ds(first, mine), :], open_ref)
    ):
        c.wait()
    tok, width = q_ref.shape
    kd = 128
    heads = width // kd
    vd = v_ref.shape[1] // heads
    scale = kd ** (-0.5)
    for h in range(heads):
        cols = slice(h * kd, (h + 1) * kd)
        vcols = slice(h * vd, (h + 1) * vd)
        for i in range(tok // BLOCK):
            lo, hi = i * BLOCK, (i + 1) * BLOCK
            q = q_ref[lo:hi, cols].astype(F32) * scale
            cum = cum_ref[lo:hi, cols]
            far_ref[lo:hi, cols] = (q * jnp.exp(cum)).astype(BF16)
            if i:
                base = cum_ref[lo - 1 : lo, cols]
                q_in = (q * jnp.exp(cum - base)).astype(BF16)
                k_in = (k_ref[0:hi, cols].astype(F32) * jnp.exp(base - cum_ref[0:hi, cols])).astype(BF16)
            else:
                q_in = (q * jnp.exp(cum)).astype(BF16)
                k_in = (k_ref[0:hi, cols].astype(F32) * jnp.exp(-cum)).astype(BF16)
            scores = dot(q_in, k_in, NT)
            seen = (
                lax.broadcasted_iota(jnp.int32, (BLOCK, hi), 0) + lo
                >= lax.broadcasted_iota(jnp.int32, (BLOCK, hi), 1)
            )
            scores = jnp.where(seen, scores, 0.0).astype(BF16)
            inside_ref[lo:hi, vcols] = dot(scores, v_ref[0:hi, vcols])


def chain_kernel(got_ref, open_ref, out_ref):
    group = got_ref.shape[0]
    rows, vd = open_ref.shape
    wide = vd // 128
    where = lax.broadcasted_iota(jnp.int32, (8, 128), 0)
    parts = []
    for g in range(group // 8):
        table = jnp.zeros((8, 128), F32)
        for d in range(8):
            pair = got_ref[g * 8 + d, wide * rows : wide * rows + 8, :].astype(F32)
            table = jnp.where(where == d, pair + pltpu.roll(pair, 1, 0), table)
        parts.append(table)
    rates = jnp.transpose(jnp.concatenate(parts, axis=0))
    states = [open_ref[:, w * 128 : (w + 1) * 128] for w in range(wide)]
    for d in range(group):
        rate = jnp.broadcast_to(rates[0:rows, d : d + 1], (rows, 128))
        for w in range(wide):
            out_ref[d, :, w * 128 : (w + 1) * 128] = states[w].astype(BF16)
            states[w] = rate * states[w] + got_ref[d, w * rows : (w + 1) * rows, :].astype(F32)


def project_kernel(who_ref, inside_ref, far_ref, start_ref, *refs):
    gain_hbm, mine, other, out_hbm = refs[0], refs[1:5], refs[5], refs[6]
    normed, weight, gain_ref, tiles, in_sems, out_sems = refs[7:]
    core, color = who_ref[1], who_ref[2]
    half = normed.shape[1] // 2
    piece = half // 4
    model = weight.shape[0]
    heads = 4
    kd, vd = far_ref.shape[1] // heads, start_ref.shape[1]
    halves = TILES
    rows = model // halves
    pairs = [(gain_hbm, gain_ref)]
    for part in range(halves):
        span = pl.ds(part * rows, rows)
        for n in range(4):
            at = lax.rem(color + n, 4) * piece
            for base, src in ((core * half, mine[n]), ((1 - core) * half, other.at[n])):
                to = pl.ds(pl.multiple_of(base + at, piece), piece)
                pairs.append((src.at[span, :], weight.at[span, to]))
    copies = fetch(in_sems, *pairs)
    copies[0].wait()
    for h in range(heads):
        o = inside_ref[:, h * vd : (h + 1) * vd] + dot(
            far_ref[:, h * kd : (h + 1) * kd], start_ref[h * kd : (h + 1) * kd, :]
        )
        spread = lax.rsqrt(jnp.mean(o * o, axis=-1, keepdims=True) + norm_eps)
        normed[:, h * vd : (h + 1) * vd] = (o * spread * gain_ref[...]).astype(BF16)
    tile = model // TILES
    outs = []
    for t in range(TILES):
        if t % (TILES // halves) == 0:
            part = t // (TILES // halves)
            for c in copies[1 + 8 * part : 9 + 8 * part]:
                c.wait()
        tiles[t] = dot(normed[...], weight[t * tile : (t + 1) * tile, :], NT).astype(BF16)
        c = pltpu.make_async_copy(tiles.at[t], out_hbm.at[:, pl.ds(t * tile, tile)], out_sems.at[t])
        c.start()
        outs.append(c)
    for c in outs:
        c.wait()


def hbm(*arrays):
    return [pltpu.with_memory_space_constraint(a, pltpu.HBM) for a in arrays]


def vmem(*arrays):
    return [pltpu.with_memory_space_constraint(a, pltpu.VMEM) for a in arrays]


def params(mib):
    return pltpu.CompilerParams(vmem_limit_bytes=mib * 2**20)


def cost(flops):
    return pl.CostEstimate(flops=flops, bytes_accessed=10**6, transcendentals=0)


def on_device(
    queries,
    head_keys,
    decay_preact,
    values,
    extra_log_decay,
    decay_offset_bias,
    opening_state,
    output_norm_gain,
    output_weight,
):
    tok, seqs, width = queries.shape
    heads, kd = decay_offset_bias.shape
    vd = output_norm_gain.shape[0]
    group = lax.axis_size("sp")
    plane = lax.axis_size("dp")
    share = output_weight.shape[1]
    model = share * plane
    piece = heads * vd // 8
    rows = heads * kd // group
    packed = rows * vd // 128 + 8
    sp, dp = lax.axis_index("sp"), lax.axis_index("dp")
    z, y = lax.div(dp, SIDE), lax.rem(dp, SIDE)
    who = jnp.stack([sp, lax.rem(sp, 2), lax.rem(y + 2 * z, 4), z]).astype(jnp.int32)
    dma = pltpu.SemaphoreType.DMA

    q = queries.reshape(tok, width)
    k = head_keys.reshape(tok, width)
    x = decay_preact.reshape(tok, width)
    v = values.reshape(tok, heads * vd)
    opening = opening_state.reshape(heads * kd, vd)

    def from_offset(dz, dy):
        return [
            (((i + dz) % SIDE) * SIDE + (j + dy) % SIDE, i * SIDE + j)
            for i in range(plane // SIDE)
            for j in range(SIDE)
        ]

    spread = pl.pallas_call(
        spread_kernel,
        out_shape=pltpu.VMEM((plane, share, piece), BF16),
        in_specs=[SMEM, HBM],
        out_specs=VMEM,
        scratch_shapes=[pltpu.VMEM((4, share, piece), BF16), dma((4,))],
        compiler_params=params(4),
        cost_estimate=cost(10**6),
        name="spread",
    )(who, *hbm(output_weight.T))
    eighth = lax.all_to_all(spread, "dp", 0, 0, tiled=True).reshape(model, piece)
    mine = [eighth]
    for o in ((0, 1), (1, 0), (0, -1)):
        mine.append(lax.ppermute(eighth, "dp", from_offset(*o)))
    stacked = jnp.stack(mine)
    other = lax.ppermute(stacked, "sp", [(i, i ^ 1) for i in range(group)])

    send, cum = pl.pallas_call(
        summary_kernel,
        out_shape=(
            pltpu.VMEM((group, packed, 128), BF16),
            pltpu.VMEM((tok, width), F32),
        ),
        in_specs=[HBM] * 5,
        out_specs=(VMEM, VMEM),
        scratch_shapes=[
            pltpu.VMEM((tok, width), BF16),
            pltpu.VMEM((tok, width), BF16),
            pltpu.VMEM((tok, heads * vd), BF16),
            pltpu.VMEM(extra_log_decay.shape, F32),
            pltpu.VMEM((heads, kd), F32),
            dma((5,)),
        ],
        compiler_params=params(16),
        cost_estimate=cost(3 * 10**8),
        name="summary",
    )(*hbm(k, x, v, extra_log_decay, decay_offset_bias))

    got = lax.all_to_all(send, "sp", 0, 0, tiled=True)

    inside, far, own_opening = pl.pallas_call(
        inside_kernel,
        out_shape=(
            pltpu.VMEM((tok, heads * vd), F32),
            pltpu.VMEM((tok, width), BF16),
            pltpu.VMEM((rows, vd), F32),
        ),
        in_specs=[SMEM, VMEM] + [HBM] * 4,
        out_specs=(VMEM, VMEM, VMEM),
        scratch_shapes=[
            pltpu.VMEM((tok, width), BF16),
            pltpu.VMEM((tok, width), BF16),
            pltpu.VMEM((tok, heads * vd), BF16),
            dma((4,)),
        ],
        compiler_params=params(16),
        cost_estimate=cost(3 * 10**8),
        name="inside",
    )(who, *vmem(cum), *hbm(q, k, v, opening))

    starts = pl.pallas_call(
        chain_kernel,
        out_shape=pltpu.VMEM((group, rows, vd), BF16),
        in_specs=[VMEM, VMEM],
        out_specs=VMEM,
        compiler_params=params(8),
        cost_estimate=cost(10**7),
        name="chain",
    )(*vmem(got, own_opening))

    start = lax.all_to_all(starts, "sp", 0, 0, tiled=True).reshape(heads * kd, vd)

    out = pl.pallas_call(
        project_kernel,
        out_shape=jax.ShapeDtypeStruct((tok, model), BF16),
        in_specs=[SMEM] + [VMEM] * 3 + [HBM] * 6,
        out_specs=HBM,
        scratch_shapes=[
            pltpu.VMEM((tok, heads * vd), BF16),
            pltpu.VMEM((model, heads * vd), BF16),
            pltpu.VMEM((1, vd), F32),
            pltpu.VMEM((TILES, tok, model // TILES), BF16),
            dma((1 + 8 * TILES,)),
            dma((TILES,)),
        ],
        compiler_params=params(24),
        cost_estimate=cost(10**9),
        name="project",
    )(who, *vmem(inside, far, start), *hbm(output_norm_gain.reshape(1, vd), *mine, other))
    return out.reshape(tok, seqs, model)


def solution(mesh):
    return jax.shard_map(
        on_device,
        mesh=mesh,
        in_specs=(
            P("sp", "dp", None),
            P("sp", "dp", None),
            P("sp", "dp", None),
            P("sp", "dp", None),
            P("dp", "sp"),
            P(),
            P("dp", None, None, None),
            P(),
            P(None, "dp"),
        ),
        out_specs=P("sp", "dp", None),
        check_vma=False,
    )
```

time: 129 us -> 113 us (0.88)
  blocking collectives: 73 us -> 55.5 us
  starting transfers between devices: 16.1 us -> 20.7 us
  Pallas kernels: 17.2 us -> 13.8 us
  local copies, waits for them, and re-layouts: 2.53 us -> 0.01 us
  waiting for transfers between devices: 19.1 us -> 20.4 us
    all_to_all x1 -> x2, blocking collectives: 73 us -> 55.5 us  [the longest x1 41.2 us: on_device(): lax.all_to_all(spread, 'dp', 0, 0, tiled=True).reshape(model, piece)]
    ppermute x1 -> x4, waiting for transfers between devices: 0.01 us -> 11.9 us  [the longest x3 11.9 us: on_device(): mine.append(lax.ppermute(eighth, 'dp', from_offset(*o)))]
    ppermute x1 -> x4, starting transfers between devices: 5.76 us -> 13.8 us  [the longest x3 8.33 us: on_device(): mine.append(lax.ppermute(eighth, 'dp', from_offset(*o)))]
    all_to_all x1 -> x0, waiting for transfers between devices: 6.75 us -> none  [on_device(): lax.all_to_all(starts, 'sp', 0, 0, tiled=True).reshape(heads * kd, vd)]
    all_to_all x1, waiting for transfers between devices: 12.4 us -> 8.46 us  [on_device(): got = lax.all_to_all(send, 'sp', 0, 0, tiled=True)]
    all_to_all x1 -> x0, starting transfers between devices: 3.43 us -> none  [on_device(): lax.all_to_all(starts, 'sp', 0, 0, tiled=True).reshape(heads * kd, vd)]
    unnamed x8, local copies, waits for them, and re-layouts: 2.28 us -> 0.01 us
    pallas_call x3 -> x4, Pallas kernels: 10.9 us -> 8.97 us  [the longest x1 3.82 us: on_device(): pl.pallas_call(inside_kernel, out_shape=(pltpu.VMEM((tok, heads * vd), F3...]
  transfers between devices with their start and end apart: 3 -> 5, of which waited for: 2 -> 4; matrix products, arithmetic and copies ran while one was open for 0% -> 0% of each run, Pallas kernels for 8% -> 7%
where the time goes in v2:
time: 113 us; the launch traced here: 112 us
  blocking collectives  55.5 us (49%)
  starting transfers between devices  20.7 us (18%)
  waiting for transfers between devices  20.4 us (18%)
  Pallas kernels  13.8 us (12%)
  other arithmetic  1.66 us (1%)
    all_to_all x1, blocking collectives, on_device(): lax.all_to_all(spread, 'dp', 0, 0, tiled=True).reshape(model, piece)  41.2 us
    all_to_all x1, blocking collectives, on_device(): lax.all_to_all(starts, 'sp', 0, 0, tiled=True).reshape(heads * kd, vd)  14.4 us
    ppermute x3, waiting for transfers between devices, on_device(): mine.append(lax.ppermute(eighth, 'dp', from_offset(*o)))  11.9 us
    all_to_all x1, waiting for transfers between devices, on_device(): got = lax.all_to_all(send, 'sp', 0, 0, tiled=True)  8.46 us
    ppermute x3, starting transfers between devices, on_device(): mine.append(lax.ppermute(eighth, 'dp', from_offset(*o)))  8.33 us
    all_to_all x1, starting transfers between devices, on_device(): got = lax.all_to_all(send, 'sp', 0, 0, tiled=True)  6.9 us
    ppermute x1, starting transfers between devices, on_device(): other = lax.ppermute(stacked, 'sp', [(i, i ^ 1) for i in range(group)])  5.5 us
    pallas_call x1, Pallas kernels, on_device(): pl.pallas_call(project_kernel, out_shape=jax.ShapeDtypeStruct((tok, model...  4.8 us
  transfers between devices with their start and end apart: 5, of which 4 were waited for; matrix products, arithmetic and copies ran while one was open for 0% of the time, Pallas kernels for 7%

profile of v2, /device:TPU:1, one launch (start us, length us, event | category | flops | bytes accessed | tf_op | source)
XLA Modules:
  0.0 112.2 jit_solution(13938286925066934510)
XLA Ops:
  0.0 0.1 pad_add_fusion.who_ref
  0.1 1.4 %spread.1 = bf16[64,32,128]{2,1,0:T(8,128)(2,1)S(1)} custom-call(s32[4]{0:T(128)S(1)} %pad_add_fusion.who_ref, bf16[32,1024]{1,0:T(8,128)(2,1)} %bitcast.33), custom_call_target="tpu_custom_call" | custom-call | flops 1000000 | bytes 1000000 | tf_op jit(solution)/shard_map/spread/pallas_call | solution.py:253
  1.5 41.2 %all_to_all.15 = bf16[64,32,128]{2,1,0:T(8,128)(2,1)S(1)} all-to-all(bf16[64,32,128]{2,1,0:T(8,128)(2,1)S(1)} %spread.1), channel_id=1, replica_groups=mesh['sp'=16,'dp'=64] {'dp'}, dimensions={0} | all-to-all | bytes 1048576 | tf_op jit(solution)/shard_map/all_to_all | solution.py:263
  42.6 0.0 copy-start
  42.6 3.4 %collective-permute-start = (bf16[2048,128]{1,0:T(8,128)(2,1)S(1)}, bf16[2048,128]{1,0:T(8,128)(2,1)S(1)}, u32[]{:S(2)}, u32[]{:S(2)}) collective-permute-start(bf16[2048,128]{1,0:T(8,128)(2,1)S(1)} %bitcast.19), channel_id=1, source_target_pairs={{1,0},{2,1},{3,2},{4,3},{5,4},{6,5},{7,6},{0,7},{9,8},{10,9},{11,1... | collective-permute-start | bytes 1572872 | tf_op jit(solution)/shard_map/ppermute | solution.py:266
  46.0 3.0 %collective-permute-start.1 = (bf16[2048,128]{1,0:T(8,128)(2,1)S(1)}, bf16[2048,128]{1,0:T(8,128)(2,1)S(1)}, u32[]{:S(2)}, u32[]{:S(2)}) collective-permute-start(bf16[2048,128]{1,0:T(8,128)(2,1)S(1)} %bitcast.20), channel_id=1, source_target_pairs={{8,0},{9,1},{10,2},{11,3},{12,4},{13,5},{14,6},{15,7},{16,8},{17,9... | collective-permute-start | bytes 1572872 | tf_op jit(solution)/shard_map/ppermute | solution.py:266
  49.1 1.9 %collective-permute-start.2 = (bf16[2048,128]{1,0:T(8,128)(2,1)S(1)}, bf16[2048,128]{1,0:T(8,128)(2,1)S(1)}, u32[]{:S(2)}, u32[]{:S(2)}) collective-permute-start(bf16[2048,128]{1,0:T(8,128)(2,1)S(1)} %bitcast.21), channel_id=1, source_target_pairs={{7,0},{0,1},{1,2},{2,3},{3,4},{4,5},{5,6},{6,7},{15,8},{8,9},{9,10... | collective-permute-start | bytes 1572872 | tf_op jit(solution)/shard_map/ppermute | solution.py:266
  51.0 4.1 %collective-permute-done.refs_2_ = bf16[2048,128]{1,0:T(8,128)(2,1)S(1)} collective-permute-done((bf16[2048,128]{1,0:T(8,128)(2,1)S(1)}, bf16[2048,128]{1,0:T(8,128)(2,1)S(1)}, u32[]{:S(2)}, u32[]{:S(2)}) %collective-permute-start) | collective-permute-done | bytes 524320 | tf_op jit(solution)/shard_map/ppermute | solution.py:266
  55.1 3.8 %collective-permute-done.1.refs_3_ = bf16[2048,128]{1,0:T(8,128)(2,1)S(1)} collective-permute-done((bf16[2048,128]{1,0:T(8,128)(2,1)S(1)}, bf16[2048,128]{1,0:T(8,128)(2,1)S(1)}, u32[]{:S(2)}, u32[]{:S(2)}) %collective-permute-start.1) | collective-permute-done | bytes 524320 | tf_op jit(solution)/shard_map/ppermute | solution.py:266
  59.0 4.0 %collective-permute-done.2.refs_4_ = bf16[2048,128]{1,0:T(8,128)(2,1)S(1)} collective-permute-done((bf16[2048,128]{1,0:T(8,128)(2,1)S(1)}, bf16[2048,128]{1,0:T(8,128)(2,1)S(1)}, u32[]{:S(2)}, u32[]{:S(2)}) %collective-permute-start.2) | collective-permute-done | bytes 524320 | tf_op jit(solution)/shard_map/ppermute | solution.py:266
  62.9 1.6 %pad_maximum_fusion = bf16[4,2048,128]{2,1,0:T(8,128)(2,1)} fusion(bf16[1,2048,128]{2,1,0:T(8,128)(2,1)S(1)} %bitcast.26, bf16[1,2048,128]{2,1,0:T(8,128)(2,1)S(1)} %bitcast.25, bf16[1,2048,128]{2,1,0:T(8,128)(2,1)S(1)} %bitcast.24, bf16[1,2048,128]{2,1,0:T(8,128)(2,1)S(1)} %bitcast.22), kind=kLoop, calls=%fused_computation | loop fusion | flops 3145728 | bytes 4194304 | tf_op jit(solution)/shard_map/stack | solution.py:267
  64.5 0.0 copy-done
  64.5 0.0 copy-done.1
  64.5 0.0 copy-done.2
  64.5 0.0 copy-done.3
  64.5 5.5 %collective-permute-start.3 = (bf16[4,2048,128]{2,1,0:T(8,128)(2,1)}, bf16[4,2048,128]{2,1,0:T(8,128)(2,1)}, u32[]{:S(2)}, u32[]{:S(2)}) collective-permute-start(bf16[4,2048,128]{2,1,0:T(8,128)(2,1)} %pad_maximum_fusion), channel_id=1, source_target_pairs={{0,64},{64,0},{128,192},{192,128},{256,320},{320,256},{384,448},{4... | collective-permute-start | bytes 6291464 | tf_op jit(solution)/shard_map/ppermute | solution.py:268
  70.0 3.5 %summary.1 = (bf16[16,72,128]{2,1,0:T(8,128)(2,1)}, f32[256,512]{1,0:T(8,128)S(1)}) custom-call(bf16[256,512]{1,0:T(8,128)(2,1)} %bitcast.30, bf16[256,512]{1,0:T(8,128)(2,1)} %bitcast.35, bf16[256,1024]{1,0:T(8,128)(2,1)} %bitcast.27, f32[4,256]{1,0:T(4,128)} %extra_hbm.1, f32[4,128]{1,0:T(4,128)} %bias_hbm.1), custom_call_target="tpu_custom_call" | custom-call | flops 300000000 | bytes 1000000 | tf_op jit(solution)/shard_map/summary/pallas_call | solution.py:270
  73.5 6.9 %all-to-all-start = ((bf16[16,72,128]{2,1,0:T(8,128)(2,1)}), bf16[16,72,128]{2,1,0:T(8,128)(2,1)S(1)}, u32[]{:S(2)}, u32[]{:S(2)}) async-start(bf16[16,72,128]{2,1,0:T(8,128)(2,1)} %get-tuple-element.13), calls=%async_computation | async-start | bytes 589824 | tf_op jit(solution)/shard_map/all_to_all | solution.py:291
  80.4 3.8 %inside.1 = (f32[256,1024]{1,0:T(8,128)S(1)}, bf16[256,512]{1,0:T(8,128)(2,1)S(1)}, f32[32,256]{1,0:T(8,128)S(1)}) custom-call(s32[4]{0:T(128)S(1)} %pad_add_fusion.who_ref, f32[256,512]{1,0:T(8,128)S(1)} %get-tuple-element.10.cum_ref, bf16[256,512]{1,0:T(8,128)(2,1)} %bitcast.32, bf16[256,512]{1,0:T(8,128)(2,1)} %bitcast.31, bf16[256,1024]{1,0:T(8,128)(2,1)} %bitcast.28, ...), custom_call_target="tpu_custom_call" | custom-call | flops 300000000 | bytes 1000000 | tf_op jit(solution)/shard_map/inside/pallas_call | solution.py:293
  84.3 8.5 %all-to-all-done.got_ref = bf16[16,72,128]{2,1,0:T(8,128)(2,1)S(1)} async-done(((bf16[16,72,128]{2,1,0:T(8,128)(2,1)}), bf16[16,72,128]{2,1,0:T(8,128)(2,1)S(1)}, u32[]{:S(2)}, u32[]{:S(2)}) %all-to-all-start) | async-done | bytes 294944 | tf_op jit(solution)/shard_map/all_to_all | solution.py:291
  92.7 0.2 chain.1
  93.0 14.4 %all_to_all.16 = bf16[16,32,256]{2,1,0:T(8,128)(2,1)S(1)} all-to-all(bf16[16,32,256]{2,1,0:T(8,128)(2,1)S(1)} %chain.1), channel_id=1, replica_groups=mesh['sp'=16,'dp'=64] {'sp'}, dimensions={0} | all-to-all | bytes 524288 | tf_op jit(solution)/shard_map/all_to_all | solution.py:323
  107.3 0.0 collective-permute-done.3.refs_5_
  107.4 4.8 %project.1 = bf16[256,2048]{1,0:T(8,128)(2,1)} custom-call(s32[4]{0:T(128)S(1)} %pad_add_fusion.who_ref, f32[256,1024]{1,0:T(8,128)S(1)} %get-tuple-element.11.inside_ref, bf16[256,512]{1,0:T(8,128)(2,1)S(1)} %get-tuple-element.12.far_ref, bf16[512,256]{1,0:T(8,128)(2,1)S(1)} %bitcast.18, f32[1,256]{1,0:T(1,128)} %bitcast.34, bf16[2048,128]{1,0:T(8,128)(2,1)} %bitcast.23, ...), custom_call_target="tpu_custom_call" | custom-call | flops 1000000000 | bytes 1000000 | tf_op jit(solution)/shard_map/project/pallas_call | solution.py:325
  (3 shorter events, 0.0 us)
Async XLA Ops:
  42.6 21.9 %copy-start = (bf16[64,32,128]{2,1,0:T(8,128)(2,1)}, bf16[64,32,128]{2,1,0:T(8,128)(2,1)S(1)}, u32[]{:S(2)}) copy-start(bf16[64,32,128]{2,1,0:T(8,128)(2,1)S(1)} %all_to_all.15) | copy-start | bytes 1572868
  42.6 12.5 %collective-permute-start = (bf16[2048,128]{1,0:T(8,128)(2,1)S(1)}, bf16[2048,128]{1,0:T(8,128)(2,1)S(1)}, u32[]{:S(2)}, u32[]{:S(2)}) collective-permute-start(bf16[2048,128]{1,0:T(8,128)(2,1)S(1)} %bitcast.19), channel_id=1, source_target_pairs={{1,0},{2,1},{3,2},{4,3},{5,4},{6,5},{7,6},{0,7},{9,8},{10,9},{11,1... | collective-permute-start | bytes 1572872 | tf_op jit(solution)/shard_map/ppermute | solution.py:266
  46.0 12.9 %collective-permute-start.1 = (bf16[2048,128]{1,0:T(8,128)(2,1)S(1)}, bf16[2048,128]{1,0:T(8,128)(2,1)S(1)}, u32[]{:S(2)}, u32[]{:S(2)}) collective-permute-start(bf16[2048,128]{1,0:T(8,128)(2,1)S(1)} %bitcast.20), channel_id=1, source_target_pairs={{8,0},{9,1},{10,2},{11,3},{12,4},{13,5},{14,6},{15,7},{16,8},{17,9... | collective-permute-start | bytes 1572872 | tf_op jit(solution)/shard_map/ppermute | solution.py:266
  49.1 13.8 %collective-permute-start.2 = (bf16[2048,128]{1,0:T(8,128)(2,1)S(1)}, bf16[2048,128]{1,0:T(8,128)(2,1)S(1)}, u32[]{:S(2)}, u32[]{:S(2)}) collective-permute-start(bf16[2048,128]{1,0:T(8,128)(2,1)S(1)} %bitcast.21), channel_id=1, source_target_pairs={{7,0},{0,1},{1,2},{2,3},{3,4},{4,5},{5,6},{6,7},{15,8},{8,9},{9,10... | collective-permute-start | bytes 1572872 | tf_op jit(solution)/shard_map/ppermute | solution.py:266
  55.1 9.4 %copy-start.1 = (bf16[2048,128]{1,0:T(8,128)(2,1)}, bf16[2048,128]{1,0:T(8,128)(2,1)S(1)}, u32[]{:S(2)}) copy-start(bf16[2048,128]{1,0:T(8,128)(2,1)S(1)} %collective-permute-done.refs_2_) | copy-start | bytes 1572868
  59.0 5.6 %copy-start.2 = (bf16[2048,128]{1,0:T(8,128)(2,1)}, bf16[2048,128]{1,0:T(8,128)(2,1)S(1)}, u32[]{:S(2)}) copy-start(bf16[2048,128]{1,0:T(8,128)(2,1)S(1)} %collective-permute-done.1.refs_3_) | copy-start | bytes 1572868
  62.9 1.6 %copy-start.3 = (bf16[2048,128]{1,0:T(8,128)(2,1)}, bf16[2048,128]{1,0:T(8,128)(2,1)S(1)}, u32[]{:S(2)}) copy-start(bf16[2048,128]{1,0:T(8,128)(2,1)S(1)} %collective-permute-done.2.refs_4_) | copy-start | bytes 1572868
  64.5 42.8 %collective-permute-start.3 = (bf16[4,2048,128]{2,1,0:T(8,128)(2,1)}, bf16[4,2048,128]{2,1,0:T(8,128)(2,1)}, u32[]{:S(2)}, u32[]{:S(2)}) collective-permute-start(bf16[4,2048,128]{2,1,0:T(8,128)(2,1)} %pad_maximum_fusion), channel_id=1, source_target_pairs={{0,64},{64,0},{128,192},{192,128},{256,320},{320,256},{384,448},{4... | collective-permute-start | bytes 6291464 | tf_op jit(solution)/shard_map/ppermute | solution.py:268
  73.5 19.2 %all-to-all-start = ((bf16[16,72,128]{2,1,0:T(8,128)(2,1)}), bf16[16,72,128]{2,1,0:T(8,128)(2,1)S(1)}, u32[]{:S(2)}, u32[]{:S(2)}) async-start(bf16[16,72,128]{2,1,0:T(8,128)(2,1)} %get-tuple-element.13), calls=%async_computation | async-start | bytes 589824 | tf_op jit(solution)/shard_map/all_to_all | solution.py:291

commit v3 on v2

--- a/solution.py
+++ b/solution.py
@@ -154,22 +154,22 @@
 
 
 def project_kernel(who_ref, inside_ref, far_ref, start_ref, *refs):
-    gain_hbm, mine, other, out_hbm = refs[0], refs[1:5], refs[5], refs[6]
-    normed, weight, gain_ref, tiles, in_sems, out_sems = refs[7:]
+    gain_hbm, mine, other, out_hbm = refs[0], refs[1:5], refs[5:9], refs[9]
+    normed, weight, gain_ref, tiles, in_sems, out_sems = refs[10:]
     core, color = who_ref[1], who_ref[2]
     half = normed.shape[1] // 2
     piece = half // 4
     model = weight.shape[0]
     heads = 4
     kd, vd = far_ref.shape[1] // heads, start_ref.shape[1]
-    halves = TILES
+    halves = 2
     rows = model // halves
     pairs = [(gain_hbm, gain_ref)]
     for part in range(halves):
         span = pl.ds(part * rows, rows)
         for n in range(4):
             at = lax.rem(color + n, 4) * piece
-            for base, src in ((core * half, mine[n]), ((1 - core) * half, other.at[n])):
+            for base, src in ((core * half, mine[n]), ((1 - core) * half, other[n])):
                 to = pl.ds(pl.multiple_of(base + at, piece), piece)
                 pairs.append((src.at[span, :], weight.at[span, to]))
     copies = fetch(in_sems, *pairs)
@@ -264,8 +264,9 @@
     mine = [eighth]
     for o in ((0, 1), (1, 0), (0, -1)):
         mine.append(lax.ppermute(eighth, "dp", from_offset(*o)))
-    stacked = jnp.stack(mine)
-    other = lax.ppermute(stacked, "sp", [(i, i ^ 1) for i in range(group)])
+    other = []
+    for chunk in mine:
+        other.append(lax.ppermute(chunk, "sp", [(i, i ^ 1) for i in range(group)]))
 
     send, cum = pl.pallas_call(
         summary_kernel,
@@ -325,20 +326,20 @@
     out = pl.pallas_call(
         project_kernel,
         out_shape=jax.ShapeDtypeStruct((tok, model), BF16),
-        in_specs=[SMEM] + [VMEM] * 3 + [HBM] * 6,
+        in_specs=[SMEM] + [VMEM] * 3 + [HBM] * 9,
         out_specs=HBM,
         scratch_shapes=[
             pltpu.VMEM((tok, heads * vd), BF16),
             pltpu.VMEM((model, heads * vd), BF16),
             pltpu.VMEM((1, vd), F32),
             pltpu.VMEM((TILES, tok, model // TILES), BF16),
-            dma((1 + 8 * TILES,)),
+            dma((17,)),
             dma((TILES,)),
         ],
         compiler_params=params(24),
         cost_estimate=cost(10**9),
         name="project",
-    )(who, *vmem(inside, far, start), *hbm(output_norm_gain.reshape(1, vd), *mine, other))
+    )(who, *vmem(inside, far, start), *hbm(output_norm_gain.reshape(1, vd), *mine, *other))
     return out.reshape(tok, seqs, model)
 
 

time: 113 us -> 102 us (0.903)
  waiting for transfers between devices: 20.4 us -> 0.02 us
  starting transfers between devices: 20.7 us -> 28.2 us
  blocking collectives: 55.5 us -> 59.8 us
  other arithmetic: 1.66 us -> 0.08 us
    ppermute x3, waiting for transfers between devices: 11.9 us -> 0.01 us  [on_device(): mine.append(lax.ppermute(eighth, 'dp', from_offset(*o)))]
    all_to_all x1, waiting for transfers between devices: 8.46 us -> 0.01 us  [on_device(): got = lax.all_to_all(send, 'sp', 0, 0, tiled=True)]
    all_to_all x1, blocking collectives: 14.4 us -> 18.6 us  [on_device(): lax.all_to_all(starts, 'sp', 0, 0, tiled=True).reshape(heads * kd, vd)]
    all_to_all x1, starting transfers between devices: 6.9 us -> 10.6 us  [on_device(): got = lax.all_to_all(send, 'sp', 0, 0, tiled=True)]
    ppermute x1 -> x4, starting transfers between devices: 5.5 us -> 8.66 us  [on_device(): other.append(lax.ppermute(chunk, 'sp', [(i, i ^ 1) for i in range(group)]))]
    another operation x1 -> x0, other arithmetic: 1.58 us -> none  [on_device(): stacked = jnp.stack(mine)]
  transfers between devices with their start and end apart: 5 -> 8, of which waited for: 4 -> 0; matrix products, arithmetic and copies ran while one was open for 0% -> 0% of each run, Pallas kernels for 7% -> 7%
where the time goes in v3:
time: 102 us
  blocking collectives  59.8 us (59%)
  starting transfers between devices  28.2 us (28%)
  Pallas kernels  13.4 us (13%)
    all_to_all x1, blocking collectives, on_device(): lax.all_to_all(spread, 'dp', 0, 0, tiled=True).reshape(model, piece)  41.2 us
    all_to_all x1, blocking collectives, on_device(): lax.all_to_all(starts, 'sp', 0, 0, tiled=True).reshape(heads * kd, vd)  18.6 us
    all_to_all x1, starting transfers between devices, on_device(): got = lax.all_to_all(send, 'sp', 0, 0, tiled=True)  10.6 us
    ppermute x3, starting transfers between devices, on_device(): mine.append(lax.ppermute(eighth, 'dp', from_offset(*o)))  8.85 us
    ppermute x4, starting transfers between devices, on_device(): other.append(lax.ppermute(chunk, 'sp', [(i, i ^ 1) for i in range(group)]))  8.66 us
    pallas_call x1, Pallas kernels, on_device(): pl.pallas_call(project_kernel, out_shape=jax.ShapeDtypeStruct((tok, model...  4.46 us
    pallas_call x1, Pallas kernels, on_device(): pl.pallas_call(inside_kernel, out_shape=(pltpu.VMEM((tok, heads * vd), F3...  3.83 us
    pallas_call x1, Pallas kernels, on_device(): pl.pallas_call(summary_kernel, out_shape=(pltpu.VMEM((group, packed, 128)...  3.5 us
  transfers between devices with their start and end apart: 8, of which 0 were waited for; matrix products, arithmetic and copies ran while one was open for 0% of the time, Pallas kernels for 7%

profile of v3, /device:TPU:1, one launch (start us, length us, event | category | flops | bytes accessed | tf_op | source)
XLA Modules:
  0.0 101.6 jit_solution(8574226852987769865)
XLA Ops:
  0.0 0.1 pad_add_fusion.who_ref
  0.1 1.4 %spread.1 = bf16[64,32,128]{2,1,0:T(8,128)(2,1)S(1)} custom-call(s32[4]{0:T(128)S(1)} %pad_add_fusion.who_ref, bf16[32,1024]{1,0:T(8,128)(2,1)} %bitcast.26), custom_call_target="tpu_custom_call" | custom-call | flops 1000000 | bytes 1000000 | tf_op jit(solution)/shard_map/spread/pallas_call | solution.py:253
  1.5 41.2 %all_to_all.15 = bf16[64,32,128]{2,1,0:T(8,128)(2,1)S(1)} all-to-all(bf16[64,32,128]{2,1,0:T(8,128)(2,1)S(1)} %spread.1), channel_id=1, replica_groups=mesh['sp'=16,'dp'=64] {'dp'}, dimensions={0} | all-to-all | bytes 1048576 | tf_op jit(solution)/shard_map/all_to_all | solution.py:263
  42.6 3.2 %collective-permute-start.2 = (bf16[2048,128]{1,0:T(8,128)(2,1)S(1)}, bf16[2048,128]{1,0:T(8,128)(2,1)S(1)}, u32[]{:S(2)}, u32[]{:S(2)}) collective-permute-start(bf16[2048,128]{1,0:T(8,128)(2,1)S(1)} %bitcast.15), channel_id=1, source_target_pairs={{7,0},{0,1},{1,2},{2,3},{3,4},{4,5},{5,6},{6,7},{15,8},{8,9},{9,10... | collective-permute-start | bytes 1572872 | tf_op jit(solution)/shard_map/ppermute | solution.py:266
  45.8 2.5 %collective-permute-start.1 = (bf16[2048,128]{1,0:T(8,128)(2,1)S(1)}, bf16[2048,128]{1,0:T(8,128)(2,1)}, u32[]{:S(2)}, u32[]{:S(2)}) collective-permute-start(bf16[2048,128]{1,0:T(8,128)(2,1)S(1)} %bitcast.16), channel_id=1, source_target_pairs={{8,0},{9,1},{10,2},{11,3},{12,4},{13,5},{14,6},{15,7},{16,8},{17,9... | collective-permute-start | bytes 1572872 | tf_op jit(solution)/shard_map/ppermute | solution.py:266
  48.3 3.2 %collective-permute-start = (bf16[2048,128]{1,0:T(8,128)(2,1)S(1)}, bf16[2048,128]{1,0:T(8,128)(2,1)}, u32[]{:S(2)}, u32[]{:S(2)}) collective-permute-start(bf16[2048,128]{1,0:T(8,128)(2,1)S(1)} %bitcast.17), channel_id=1, source_target_pairs={{1,0},{2,1},{3,2},{4,3},{5,4},{6,5},{7,6},{0,7},{9,8},{10,9},{11,1... | collective-permute-start | bytes 1572872 | tf_op jit(solution)/shard_map/ppermute | solution.py:266
  51.5 3.5 %summary.1 = (bf16[16,72,128]{2,1,0:T(8,128)(2,1)}, f32[256,512]{1,0:T(8,128)S(1)}) custom-call(bf16[256,512]{1,0:T(8,128)(2,1)} %bitcast.23, bf16[256,512]{1,0:T(8,128)(2,1)} %bitcast.28, bf16[256,1024]{1,0:T(8,128)(2,1)} %bitcast.20, f32[4,256]{1,0:T(4,128)} %extra_hbm.1, f32[4,128]{1,0:T(4,128)} %bias_hbm.1), custom_call_target="tpu_custom_call" | custom-call | flops 300000000 | bytes 1000000 | tf_op jit(solution)/shard_map/summary/pallas_call | solution.py:271
  55.0 10.6 %all-to-all-start = ((bf16[16,72,128]{2,1,0:T(8,128)(2,1)}), bf16[16,72,128]{2,1,0:T(8,128)(2,1)S(1)}, u32[]{:S(2)}, u32[]{:S(2)}) async-start(bf16[16,72,128]{2,1,0:T(8,128)(2,1)} %get-tuple-element.13), calls=%async_computation | async-start | bytes 589824 | tf_op jit(solution)/shard_map/all_to_all | solution.py:292
  65.7 2.0 %collective-permute-start.3 = (bf16[2048,128]{1,0:T(8,128)(2,1)S(1)}, bf16[2048,128]{1,0:T(8,128)(2,1)}, u32[]{:S(2)}, u32[]{:S(2)}) collective-permute-start(bf16[2048,128]{1,0:T(8,128)(2,1)S(1)} %bitcast.18), channel_id=1, source_target_pairs={{0,64},{64,0},{128,192},{192,128},{256,320},{320,256},{384,448},{4... | collective-permute-start | bytes 1572872 | tf_op jit(solution)/shard_map/ppermute | solution.py:269
  67.7 0.0 collective-permute-done.2.refs_4_
  67.7 2.3 %collective-permute-start.6 = (bf16[2048,128]{1,0:T(8,128)(2,1)S(1)}, bf16[2048,128]{1,0:T(8,128)(2,1)}, u32[]{:S(2)}, u32[]{:S(2)}) collective-permute-start(bf16[2048,128]{1,0:T(8,128)(2,1)S(1)} %collective-permute-done.2.refs_4_), channel_id=1, source_target_pairs={{0,64},{64,0},{128,192},{192,128},{256,320},{320,256},{384,448},{4... | collective-permute-start | bytes 1572872 | tf_op jit(solution)/shard_map/ppermute | solution.py:269
  70.0 0.0 collective-permute-done.1.refs_3_
  70.1 2.0 %collective-permute-start.5 = (bf16[2048,128]{1,0:T(8,128)(2,1)}, bf16[2048,128]{1,0:T(8,128)(2,1)}, u32[]{:S(2)}, u32[]{:S(2)}) collective-permute-start(bf16[2048,128]{1,0:T(8,128)(2,1)} %collective-permute-done.1.refs_3_), channel_id=1, source_target_pairs={{0,64},{64,0},{128,192},{192,128},{256,320},{320,256},{384,448},{4... | collective-permute-start | bytes 1572872 | tf_op jit(solution)/shard_map/ppermute | solution.py:269
  72.1 0.0 collective-permute-done.refs_2_
  72.1 2.3 %collective-permute-start.4 = (bf16[2048,128]{1,0:T(8,128)(2,1)}, bf16[2048,128]{1,0:T(8,128)(2,1)}, u32[]{:S(2)}, u32[]{:S(2)}) collective-permute-start(bf16[2048,128]{1,0:T(8,128)(2,1)} %collective-permute-done.refs_2_), channel_id=1, source_target_pairs={{0,64},{64,0},{128,192},{192,128},{256,320},{320,256},{384,448},{4... | collective-permute-start | bytes 1572872 | tf_op jit(solution)/shard_map/ppermute | solution.py:269
  74.4 3.8 %inside.1 = (f32[256,1024]{1,0:T(8,128)S(1)}, bf16[256,512]{1,0:T(8,128)(2,1)S(1)}, f32[32,256]{1,0:T(8,128)S(1)}) custom-call(s32[4]{0:T(128)S(1)} %pad_add_fusion.who_ref, f32[256,512]{1,0:T(8,128)S(1)} %get-tuple-element.10.cum_ref, bf16[256,512]{1,0:T(8,128)(2,1)} %bitcast.25, bf16[256,512]{1,0:T(8,128)(2,1)} %bitcast.24, bf16[256,1024]{1,0:T(8,128)(2,1)} %bitcast.21, ...), custom_call_target="tpu_custom_call" | custom-call | flops 300000000 | bytes 1000000 | tf_op jit(solution)/shard_map/inside/pallas_call | solution.py:294
  78.3 0.0 all-to-all-done.got_ref
  78.3 0.2 chain.1
  78.5 18.6 %all_to_all.16 = bf16[16,32,256]{2,1,0:T(8,128)(2,1)S(1)} all-to-all(bf16[16,32,256]{2,1,0:T(8,128)(2,1)S(1)} %chain.1), channel_id=1, replica_groups=mesh['sp'=16,'dp'=64] {'sp'}, dimensions={0} | all-to-all | bytes 524288 | tf_op jit(solution)/shard_map/all_to_all | solution.py:324
  97.1 0.0 collective-permute-done.3.refs_5_
  97.1 0.0 collective-permute-done.6.refs_8_
  97.1 0.0 collective-permute-done.5.refs_7_
  97.1 0.0 collective-permute-done.4.refs_6_
  97.1 4.5 %project.1 = bf16[256,2048]{1,0:T(8,128)(2,1)} custom-call(s32[4]{0:T(128)S(1)} %pad_add_fusion.who_ref, f32[256,1024]{1,0:T(8,128)S(1)} %get-tuple-element.11.inside_ref, bf16[256,512]{1,0:T(8,128)(2,1)S(1)} %get-tuple-element.12.far_ref, bf16[512,256]{1,0:T(8,128)(2,1)S(1)} %bitcast.14, f32[1,256]{1,0:T(1,128)} %bitcast.27, bf16[2048,128]{1,0:T(8,128)(2,1)} %bitcast.19, ...), custom_call_target="tpu_custom_call" | custom-call | flops 1000000000 | bytes 1000000 | tf_op jit(solution)/shard_map/project/pallas_call | solution.py:326
  (4 shorter events, 0.0 us)
Async XLA Ops:
  42.6 23.0 %copy-start = (bf16[64,32,128]{2,1,0:T(8,128)(2,1)}, bf16[64,32,128]{2,1,0:T(8,128)(2,1)S(1)}, u32[]{:S(2)}) copy-start(bf16[64,32,128]{2,1,0:T(8,128)(2,1)S(1)} %all_to_all.15) | copy-start | bytes 1572868
  42.6 25.1 %collective-permute-start.2 = (bf16[2048,128]{1,0:T(8,128)(2,1)S(1)}, bf16[2048,128]{1,0:T(8,128)(2,1)S(1)}, u32[]{:S(2)}, u32[]{:S(2)}) collective-permute-start(bf16[2048,128]{1,0:T(8,128)(2,1)S(1)} %bitcast.15), channel_id=1, source_target_pairs={{7,0},{0,1},{1,2},{2,3},{3,4},{4,5},{5,6},{6,7},{15,8},{8,9},{9,10... | collective-permute-start | bytes 1572872 | tf_op jit(solution)/shard_map/ppermute | solution.py:266
  45.8 24.2 %collective-permute-start.1 = (bf16[2048,128]{1,0:T(8,128)(2,1)S(1)}, bf16[2048,128]{1,0:T(8,128)(2,1)}, u32[]{:S(2)}, u32[]{:S(2)}) collective-permute-start(bf16[2048,128]{1,0:T(8,128)(2,1)S(1)} %bitcast.16), channel_id=1, source_target_pairs={{8,0},{9,1},{10,2},{11,3},{12,4},{13,5},{14,6},{15,7},{16,8},{17,9... | collective-permute-start | bytes 1572872 | tf_op jit(solution)/shard_map/ppermute | solution.py:266
  48.3 23.7 %collective-permute-start = (bf16[2048,128]{1,0:T(8,128)(2,1)S(1)}, bf16[2048,128]{1,0:T(8,128)(2,1)}, u32[]{:S(2)}, u32[]{:S(2)}) collective-permute-start(bf16[2048,128]{1,0:T(8,128)(2,1)S(1)} %bitcast.17), channel_id=1, source_target_pairs={{1,0},{2,1},{3,2},{4,3},{5,4},{6,5},{7,6},{0,7},{9,8},{10,9},{11,1... | collective-permute-start | bytes 1572872 | tf_op jit(solution)/shard_map/ppermute | solution.py:266
  55.0 23.2 %all-to-all-start = ((bf16[16,72,128]{2,1,0:T(8,128)(2,1)}), bf16[16,72,128]{2,1,0:T(8,128)(2,1)S(1)}, u32[]{:S(2)}, u32[]{:S(2)}) async-start(bf16[16,72,128]{2,1,0:T(8,128)(2,1)} %get-tuple-element.13), calls=%async_computation | async-start | bytes 589824 | tf_op jit(solution)/shard_map/all_to_all | solution.py:292
  65.7 31.4 %collective-permute-start.3 = (bf16[2048,128]{1,0:T(8,128)(2,1)S(1)}, bf16[2048,128]{1,0:T(8,128)(2,1)}, u32[]{:S(2)}, u32[]{:S(2)}) collective-permute-start(bf16[2048,128]{1,0:T(8,128)(2,1)S(1)} %bitcast.18), channel_id=1, source_target_pairs={{0,64},{64,0},{128,192},{192,128},{256,320},{320,256},{384,448},{4... | collective-permute-start | bytes 1572872 | tf_op jit(solution)/shard_map/ppermute | solution.py:269
  67.7 10.5 %copy-start.1 = (bf16[2048,128]{1,0:T(8,128)(2,1)}, bf16[2048,128]{1,0:T(8,128)(2,1)S(1)}, u32[]{:S(2)}) copy-start(bf16[2048,128]{1,0:T(8,128)(2,1)S(1)} %collective-permute-done.2.refs_4_) | copy-start | bytes 1572868
  67.7 29.4 %collective-permute-start.6 = (bf16[2048,128]{1,0:T(8,128)(2,1)S(1)}, bf16[2048,128]{1,0:T(8,128)(2,1)}, u32[]{:S(2)}, u32[]{:S(2)}) collective-permute-start(bf16[2048,128]{1,0:T(8,128)(2,1)S(1)} %collective-permute-done.2.refs_4_), channel_id=1, source_target_pairs={{0,64},{64,0},{128,192},{192,128},{256,320},{320,256},{384,448},{4... | collective-permute-start | bytes 1572872 | tf_op jit(solution)/shard_map/ppermute | solution.py:269
  70.1 27.1 %collective-permute-start.5 = (bf16[2048,128]{1,0:T(8,128)(2,1)}, bf16[2048,128]{1,0:T(8,128)(2,1)}, u32[]{:S(2)}, u32[]{:S(2)}) collective-permute-start(bf16[2048,128]{1,0:T(8,128)(2,1)} %collective-permute-done.1.refs_3_), channel_id=1, source_target_pairs={{0,64},{64,0},{128,192},{192,128},{256,320},{320,256},{384,448},{4... | collective-permute-start | bytes 1572872 | tf_op jit(solution)/shard_map/ppermute | solution.py:269
  72.1 25.1 %collective-permute-start.4 = (bf16[2048,128]{1,0:T(8,128)(2,1)}, bf16[2048,128]{1,0:T(8,128)(2,1)}, u32[]{:S(2)}, u32[]{:S(2)}) collective-permute-start(bf16[2048,128]{1,0:T(8,128)(2,1)} %collective-permute-done.refs_2_), channel_id=1, source_target_pairs={{0,64},{64,0},{128,192},{192,128},{256,320},{320,256},{384,448},{4... | collective-permute-start | bytes 1572872 | tf_op jit(solution)/shard_map/ppermute | solution.py:269

commit v4 on v3

--- a/solution.py
+++ b/solution.py
@@ -24,6 +24,41 @@
 
 NT = (((1,), (1,)), ((), ()))
 TN = (((0,), (0,)), ((), ()))
+
+
+def two_parts(rate):
+    coarse = rate.astype(BF16).astype(F32)
+    odd = lax.broadcasted_iota(jnp.int32, rate.shape, 0) % 2 == 1
+    return jnp.where(odd, rate - coarse, coarse).astype(BF16)
+
+
+def rate_table(pieces):
+    where = lax.broadcasted_iota(jnp.int32, (8, 128), 0)
+    table = jnp.zeros((8, 128), F32)
+    for d, piece in enumerate(pieces):
+        pair = piece.astype(F32)
+        table = jnp.where(where == d, pair + pltpu.roll(pair, 1, 0), table)
+    return table
+
+
+def combine_kernel(who_ref, own_ref, other_ref, send_ref):
+    core = who_ref[1]
+    chips, packed, lanes = send_ref.shape
+    data = packed - 8
+    rows = data // 2
+    own = own_ref[pl.ds(core * chips, chips)]
+    other = other_ref[pl.ds(core * chips, chips)]
+    early = jnp.where(core == 0, own.astype(F32), other.astype(F32))
+    late = jnp.where(core == 0, other.astype(F32), own.astype(F32))
+    late_rates = rate_table([late[n, data:] for n in range(chips)])
+    rates = late_rates * rate_table([early[n, data:] for n in range(chips)])
+    turned = jnp.transpose(late_rates)
+    for n in range(chips):
+        rate = jnp.broadcast_to(turned[0:rows, n : n + 1], (rows, lanes))
+        for w in range(2):
+            at = slice(w * rows, (w + 1) * rows)
+            send_ref[n, at, :] = (rate * early[n, at] + late[n, at]).astype(BF16)
+        send_ref[n, data:, :] = two_parts(jnp.broadcast_to(rates[n : n + 1, :], (8, lanes)))
 
 
 def fetch(sems, *pairs):
@@ -53,13 +88,13 @@
     tok = k_ref.shape[0]
     heads, kd = bias_ref.shape
     vd = v_ref.shape[1] // heads
-    per, rows = send_ref.shape[0] // heads, kd * heads // send_ref.shape[0]
+    group = send_ref.shape[0] - 1
+    per, rows = group // heads, kd * heads // group
     wide = vd // kd
     tri = (
         lax.broadcasted_iota(jnp.int32, (tok, tok), 0)
         >= lax.broadcasted_iota(jnp.int32, (tok, tok), 1)
     ).astype(BF16)
-    odd = lax.broadcasted_iota(jnp.int32, (8, kd), 0) % 2 == 1
     get_extra.wait()
     spikes = jnp.transpose(extra_ref[...])
     get_bias.wait()
@@ -82,22 +117,22 @@
         k_out = (k_ref[:, cols].astype(F32) * jnp.exp(total - cum)).astype(BF16)
         final = dot(k_out, v_ref[:, h * vd : (h + 1) * vd], TN).astype(BF16)
         rate = jnp.broadcast_to(jnp.exp(total), (8, kd))
+        send_ref[group, 16 * h : 16 * h + 8, :] = two_parts(rate)
         for r in range(per):
             for w in range(wide):
                 send_ref[h * per + r, w * rows : (w + 1) * rows, :] = final[
                     r * rows : (r + 1) * rows, w * kd : (w + 1) * kd
                 ]
             turned = pltpu.roll(rate, (kd - r * rows) % kd, 1) if r else rate
-            coarse = turned.astype(BF16).astype(F32)
-            send_ref[h * per + r, wide * rows : wide * rows + 8, :] = jnp.where(
-                odd, turned - coarse, coarse
-            ).astype(BF16)
+            send_ref[h * per + r, wide * rows : wide * rows + 8, :] = two_parts(turned)
 
 
 def inside_kernel(
-    who_ref, cum_ref, q_hbm, k_hbm, v_hbm, open_hbm, inside_ref, far_ref, open_ref, q_ref, k_ref, v_ref, sems
+    who_ref, cum_ref, other_ref, q_hbm, k_hbm, v_hbm, open_hbm, inside_ref, far_ref, open_ref, q_ref, k_ref, v_ref, sems
 ):
     mine = open_ref.shape[0]
+    second = who_ref[1] == 1
+    group = other_ref.shape[0] - 1
     first = pl.multiple_of(who_ref[0] * mine, mine)
     for c in fetch(
         sems, (q_hbm, q_ref), (k_hbm, k_ref), (v_hbm, v_ref), (open_hbm.at[pl.ds(first, mine), :], open_ref)
@@ -111,11 +146,23 @@
     for h in range(heads):
         cols = slice(h * kd, (h + 1) * kd)
         vcols = slice(h * vd, (h + 1) * vd)
+        pair = other_ref[group, 16 * h : 16 * h + 8, :].astype(F32)
+        rate = jnp.where(second, pair[0:1, :] + pair[1:2, :], 1.0)
+        blocks = range(group * h // heads, group * (h + 1) // heads)
+        before = jnp.concatenate(
+            [
+                jnp.concatenate([other_ref[b, w * mine : (w + 1) * mine, :] for b in blocks], axis=0)
+                for w in range(vd // kd)
+            ],
+            axis=1,
+        )
+        before = jnp.where(second, before.astype(F32), 0.0).astype(BF16)
         for i in range(tok // BLOCK):
             lo, hi = i * BLOCK, (i + 1) * BLOCK
             q = q_ref[lo:hi, cols].astype(F32) * scale
             cum = cum_ref[lo:hi, cols]
-            far_ref[lo:hi, cols] = (q * jnp.exp(cum)).astype(BF16)
+            far = q * jnp.exp(cum)
+            far_ref[lo:hi, cols] = (far * rate).astype(BF16)
             if i:
                 base = cum_ref[lo - 1 : lo, cols]
                 q_in = (q * jnp.exp(cum - base)).astype(BF16)
@@ -129,27 +176,21 @@
                 >= lax.broadcasted_iota(jnp.int32, (BLOCK, hi), 1)
             )
             scores = jnp.where(seen, scores, 0.0).astype(BF16)
-            inside_ref[lo:hi, vcols] = dot(scores, v_ref[0:hi, vcols])
+            inside_ref[lo:hi, vcols] = dot(scores, v_ref[0:hi, vcols]) + dot(far.astype(BF16), before)
 
 
 def chain_kernel(got_ref, open_ref, out_ref):
-    group = got_ref.shape[0]
+    chips, packed, lanes = got_ref.shape
     rows, vd = open_ref.shape
-    wide = vd // 128
-    where = lax.broadcasted_iota(jnp.int32, (8, 128), 0)
-    parts = []
-    for g in range(group // 8):
-        table = jnp.zeros((8, 128), F32)
-        for d in range(8):
-            pair = got_ref[g * 8 + d, wide * rows : wide * rows + 8, :].astype(F32)
-            table = jnp.where(where == d, pair + pltpu.roll(pair, 1, 0), table)
-        parts.append(table)
-    rates = jnp.transpose(jnp.concatenate(parts, axis=0))
-    states = [open_ref[:, w * 128 : (w + 1) * 128] for w in range(wide)]
-    for d in range(group):
-        rate = jnp.broadcast_to(rates[0:rows, d : d + 1], (rows, 128))
+    wide = vd // lanes
+    rates = jnp.transpose(rate_table([got_ref[d, packed - 8 :, :] for d in range(chips)]))
+    states = [open_ref[:, w * lanes : (w + 1) * lanes] for w in range(wide)]
+    for d in range(chips):
+        rate = jnp.broadcast_to(rates[0:rows, d : d + 1], (rows, lanes))
         for w in range(wide):
-            out_ref[d, :, w * 128 : (w + 1) * 128] = states[w].astype(BF16)
+            rounded = states[w].astype(BF16)
+            for c in range(2):
+                out_ref[2 * d + c, :, w * lanes : (w + 1) * lanes] = rounded
             states[w] = rate * states[w] + got_ref[d, w * rows : (w + 1) * rows, :].astype(F32)
 
 
@@ -161,7 +202,8 @@
     piece = half // 4
     model = weight.shape[0]
     heads = 4
-    kd, vd = far_ref.shape[1] // heads, start_ref.shape[1]
+    kd, vd = far_ref.shape[1] // heads, start_ref.shape[2]
+    group = start_ref.shape[0]
     halves = 2
     rows = model // halves
     pairs = [(gain_hbm, gain_ref)]
@@ -175,9 +217,9 @@
     copies = fetch(in_sems, *pairs)
     copies[0].wait()
     for h in range(heads):
-        o = inside_ref[:, h * vd : (h + 1) * vd] + dot(
-            far_ref[:, h * kd : (h + 1) * kd], start_ref[h * kd : (h + 1) * kd, :]
-        )
+        blocks = range(group * h // heads, group * (h + 1) // heads)
+        start = jnp.concatenate([start_ref[2 * (b % SIDE) + b // SIDE] for b in blocks], axis=0)
+        o = inside_ref[:, h * vd : (h + 1) * vd] + dot(far_ref[:, h * kd : (h + 1) * kd], start)
         spread = lax.rsqrt(jnp.mean(o * o, axis=-1, keepdims=True) + norm_eps)
         normed[:, h * vd : (h + 1) * vd] = (o * spread * gain_ref[...]).astype(BF16)
     tile = model // TILES
@@ -234,7 +276,9 @@
     packed = rows * vd // 128 + 8
     sp, dp = lax.axis_index("sp"), lax.axis_index("dp")
     z, y = lax.div(dp, SIDE), lax.rem(dp, SIDE)
-    who = jnp.stack([sp, lax.rem(sp, 2), lax.rem(y + 2 * z, 4), z]).astype(jnp.int32)
+    chip, core = lax.div(sp, 2), lax.rem(sp, 2)
+    block = core * (group // 2) + chip
+    who = jnp.stack([block, core, lax.rem(y + 2 * z, 4)]).astype(jnp.int32)
     dma = pltpu.SemaphoreType.DMA
 
     q = queries.reshape(tok, width)
@@ -268,10 +312,10 @@
     for chunk in mine:
         other.append(lax.ppermute(chunk, "sp", [(i, i ^ 1) for i in range(group)]))
 
-    send, cum = pl.pallas_call(
+    final, cum = pl.pallas_call(
         summary_kernel,
         out_shape=(
-            pltpu.VMEM((group, packed, 128), BF16),
+            pltpu.VMEM((group + 1, packed, 128), BF16),
             pltpu.VMEM((tok, width), F32),
         ),
         in_specs=[HBM] * 5,
@@ -289,7 +333,18 @@
         name="summary",
     )(*hbm(k, x, v, extra_log_decay, decay_offset_bias))
 
-    got = lax.all_to_all(send, "sp", 0, 0, tiled=True)
+    other_final = lax.ppermute(final, "sp", [(i, i ^ 1) for i in range(group)])
+    send = pl.pallas_call(
+        combine_kernel,
+        out_shape=pltpu.VMEM((group // 2, packed, 128), BF16),
+        in_specs=[SMEM, VMEM, VMEM],
+        out_specs=VMEM,
+        compiler_params=params(8),
+        cost_estimate=cost(10**7),
+        name="combine",
+    )(who, *vmem(final, other_final))
+    chips = [[2 * i + c for i in range(group // 2)] for c in range(2)]
+    got = lax.all_to_all(send, "sp", 0, 0, axis_index_groups=chips, tiled=True)
 
     inside, far, own_opening = pl.pallas_call(
         inside_kernel,
@@ -298,7 +353,7 @@
             pltpu.VMEM((tok, width), BF16),
             pltpu.VMEM((rows, vd), F32),
         ),
-        in_specs=[SMEM, VMEM] + [HBM] * 4,
+        in_specs=[SMEM, VMEM, VMEM] + [HBM] * 4,
         out_specs=(VMEM, VMEM, VMEM),
         scratch_shapes=[
             pltpu.VMEM((tok, width), BF16),
@@ -309,7 +364,7 @@
         compiler_params=params(16),
         cost_estimate=cost(3 * 10**8),
         name="inside",
-    )(who, *vmem(cum), *hbm(q, k, v, opening))
+    )(who, *vmem(cum, other_final), *hbm(q, k, v, opening))
 
     starts = pl.pallas_call(
         chain_kernel,
@@ -321,7 +376,7 @@
         name="chain",
     )(*vmem(got, own_opening))
 
-    start = lax.all_to_all(starts, "sp", 0, 0, tiled=True).reshape(heads * kd, vd)
+    start = lax.all_to_all(starts, "sp", 0, 0, tiled=True)
 
     out = pl.pallas_call(
         project_kernel,

time: 102 us -> 100 us (0.980)
  blocking collectives: 59.8 us -> 19.1 us
  starting transfers between devices: 28.2 us -> 54.5 us
  waiting for transfers between devices: 0.02 us -> 11.8 us
    all_to_all x2 -> x1, blocking collectives: 59.8 us -> 19.1 us  [on_device(): start = lax.all_to_all(starts, 'sp', 0, 0, tiled=True)]
    all_to_all x1 -> x2, starting transfers between devices: 10.6 us -> 30.4 us  [the longest x1 24 us: on_device(): lax.all_to_all(spread, 'dp', 0, 0, tiled=True).reshape(model, piece)]
    all_to_all x1 -> x2, waiting for transfers between devices: 0.01 us -> 11.8 us  [the longest x1 11.8 us: on_device(): lax.all_to_all(spread, 'dp', 0, 0, tiled=True).reshape(model, piece)]
    ppermute x4, starting transfers between devices: 8.66 us -> 12.3 us  [on_device(): other.append(lax.ppermute(chunk, 'sp', [(i, i ^ 1) for i in range(group)]))]
    ppermute x0 -> x1, starting transfers between devices: none -> 2.86 us  [on_device(): other_final = lax.ppermute(final, 'sp', [(i, i ^ 1) for i in range(group)])]
    pallas_call x1 -> x2, Pallas kernels: 3.5 us -> 4.21 us  [the longest x1 2.79 us: on_device(): pl.pallas_call(summary_kernel, out_shape=(pltpu.VMEM((group + 1, packed,...]
  transfers between devices with their start and end apart: 8 -> 10, of which waited for: 0 -> 1; matrix products, arithmetic and copies ran while one was open for 0% -> 0% of each run, Pallas kernels for 7% -> 7%
where the time goes in v4:
time: 100 us; the launch traced here: 99.6 us
  starting transfers between devices  54.5 us (54%)
  blocking collectives  19.1 us (19%)
  Pallas kernels  14.1 us (14%)
  waiting for transfers between devices  11.8 us (12%)
    all_to_all x1, starting transfers between devices, on_device(): lax.all_to_all(spread, 'dp', 0, 0, tiled=True).reshape(model, piece)  24 us
    all_to_all x1, blocking collectives, on_device(): start = lax.all_to_all(starts, 'sp', 0, 0, tiled=True)  19.1 us
    ppermute x4, starting transfers between devices, on_device(): other.append(lax.ppermute(chunk, 'sp', [(i, i ^ 1) for i in range(group)]))  12.3 us
    all_to_all x1, waiting for transfers between devices, on_device(): lax.all_to_all(spread, 'dp', 0, 0, tiled=True).reshape(model, piece)  11.8 us
    ppermute x3, starting transfers between devices, on_device(): mine.append(lax.ppermute(eighth, 'dp', from_offset(*o)))  8.85 us
    all_to_all x1, starting transfers between devices, on_device(): got = lax.all_to_all(send, 'sp', 0, 0, axis_index_groups=chips, tiled=True)  6.48 us
    pallas_call x1, Pallas kernels, on_device(): pl.pallas_call(project_kernel, out_shape=jax.ShapeDtypeStruct((tok, model...  4.46 us
    pallas_call x1, Pallas kernels, on_device(): pl.pallas_call(inside_kernel, out_shape=(pltpu.VMEM((tok, heads * vd), F3...  3.01 us
  transfers between devices with their start and end apart: 10, of which 1 were waited for; matrix products, arithmetic and copies ran while one was open for 0% of the time, Pallas kernels for 7%

profile of v4, /device:TPU:1, one launch (start us, length us, event | category | flops | bytes accessed | tf_op | source)
XLA Modules:
  0.0 99.6 jit_solution(14148342921886559227)
XLA Ops:
  0.0 0.1 pad_add_fusion.who_ref
  0.1 2.2 %spread.1 = bf16[64,32,128]{2,1,0:T(8,128)(2,1)} custom-call(s32[3]{0:T(128)S(1)} %pad_add_fusion.who_ref, bf16[32,1024]{1,0:T(8,128)(2,1)} %bitcast.23), custom_call_target="tpu_custom_call" | custom-call | flops 1000000 | bytes 1000000 | tf_op jit(solution)/shard_map/spread/pallas_call | solution.py:297
  2.3 24.0 %all-to-all-start.2 = ((bf16[64,32,128]{2,1,0:T(8,128)(2,1)}), bf16[64,32,128]{2,1,0:T(8,128)(2,1)S(1)}, u32[]{:S(2)}, u32[]{:S(2)}) async-start(bf16[64,32,128]{2,1,0:T(8,128)(2,1)} %spread.1), calls=%async_computation.2 | async-start | bytes 1048576 | tf_op jit(solution)/shard_map/all_to_all | solution.py:307
  26.2 2.8 %summary.1 = (bf16[17,72,128]{2,1,0:T(8,128)(2,1)S(1)}, f32[256,512]{1,0:T(8,128)S(1)}) custom-call(bf16[256,512]{1,0:T(8,128)(2,1)} %bitcast.20, bf16[256,512]{1,0:T(8,128)(2,1)} %bitcast.25, bf16[256,1024]{1,0:T(8,128)(2,1)} %bitcast.17, f32[4,256]{1,0:T(4,128)} %extra_hbm.1, f32[4,128]{1,0:T(4,128)} %bias_hbm.1), custom_call_target="tpu_custom_call" | custom-call | flops 300000000 | bytes 1000000 | tf_op jit(solution)/shard_map/summary/pallas_call | solution.py:315
  29.0 2.9 %collective-permute-start = (bf16[17,72,128]{2,1,0:T(8,128)(2,1)S(1)}, bf16[17,72,128]{2,1,0:T(8,128)(2,1)S(1)}, u32[]{:S(2)}, u32[]{:S(2)}) collective-permute-start(bf16[17,72,128]{2,1,0:T(8,128)(2,1)S(1)} %get-tuple-element.11.own_ref), channel_id=1, source_target_pairs={{0,64},{64,0},{128,192},{192,128},{256,320},{320,256},{384,448},{4... | collective-permute-start | bytes 940040 | tf_op jit(solution)/shard_map/ppermute | solution.py:336
  31.9 11.8 %all-to-all-done.2 = bf16[64,32,128]{2,1,0:T(8,128)(2,1)S(1)} async-done(((bf16[64,32,128]{2,1,0:T(8,128)(2,1)}), bf16[64,32,128]{2,1,0:T(8,128)(2,1)S(1)}, u32[]{:S(2)}, u32[]{:S(2)}) %all-to-all-start.2) | async-done | bytes 524320 | tf_op jit(solution)/shard_map/all_to_all | solution.py:307
  43.7 3.2 %collective-permute-start.3 = (bf16[2048,128]{1,0:T(8,128)(2,1)S(1)}, bf16[2048,128]{1,0:T(8,128)(2,1)S(1)}, u32[]{:S(2)}, u32[]{:S(2)}) collective-permute-start(bf16[2048,128]{1,0:T(8,128)(2,1)S(1)} %bitcast.12), channel_id=1, source_target_pairs={{7,0},{0,1},{1,2},{2,3},{3,4},{4,5},{5,6},{6,7},{15,8},{8,9},{9,10... | collective-permute-start | bytes 1572872 | tf_op jit(solution)/shard_map/ppermute | solution.py:310
  46.8 2.5 %collective-permute-start.2 = (bf16[2048,128]{1,0:T(8,128)(2,1)S(1)}, bf16[2048,128]{1,0:T(8,128)(2,1)}, u32[]{:S(2)}, u32[]{:S(2)}) collective-permute-start(bf16[2048,128]{1,0:T(8,128)(2,1)S(1)} %bitcast.13), channel_id=1, source_target_pairs={{8,0},{9,1},{10,2},{11,3},{12,4},{13,5},{14,6},{15,7},{16,8},{17,9... | collective-permute-start | bytes 1572872 | tf_op jit(solution)/shard_map/ppermute | solution.py:310
  49.3 3.2 %collective-permute-start.1 = (bf16[2048,128]{1,0:T(8,128)(2,1)S(1)}, bf16[2048,128]{1,0:T(8,128)(2,1)}, u32[]{:S(2)}, u32[]{:S(2)}) collective-permute-start(bf16[2048,128]{1,0:T(8,128)(2,1)S(1)} %bitcast.14), channel_id=1, source_target_pairs={{1,0},{2,1},{3,2},{4,3},{5,4},{6,5},{7,6},{0,7},{9,8},{10,9},{11,1... | collective-permute-start | bytes 1572872 | tf_op jit(solution)/shard_map/ppermute | solution.py:310
  52.5 1.4 %combine.1 = bf16[8,72,128]{2,1,0:T(8,128)(2,1)} custom-call(s32[3]{0:T(128)S(1)} %pad_add_fusion.who_ref, bf16[17,72,128]{2,1,0:T(8,128)(2,1)S(1)} %get-tuple-element.11.own_ref, bf16[17,72,128]{2,1,0:T(8,128)(2,1)S(1)} %collective-permute-done.other_ref), custom_call_target="tpu_custom_call" | custom-call | flops 10000000 | bytes 1000000 | tf_op jit(solution)/shard_map/combine/pallas_call | solution.py:337
  54.0 6.5 %all-to-all-start = ((bf16[8,72,128]{2,1,0:T(8,128)(2,1)}), bf16[8,72,128]{2,1,0:T(8,128)(2,1)S(1)}, u32[]{:S(2)}, u32[]{:S(2)}) async-start(bf16[8,72,128]{2,1,0:T(8,128)(2,1)} %combine.1), calls=%async_computation | async-start | bytes 294912 | tf_op jit(solution)/shard_map/all_to_all | solution.py:347
  60.5 6.0 %collective-permute-start.4 = (bf16[2048,128]{1,0:T(8,128)(2,1)S(1)}, bf16[2048,128]{1,0:T(8,128)(2,1)}, u32[]{:S(2)}, u32[]{:S(2)}) collective-permute-start(bf16[2048,128]{1,0:T(8,128)(2,1)S(1)} %bitcast.15), channel_id=1, source_target_pairs={{0,64},{64,0},{128,192},{192,128},{256,320},{320,256},{384,448},{4... | collective-permute-start | bytes 1572872 | tf_op jit(solution)/shard_map/ppermute | solution.py:313
  66.5 0.0 collective-permute-done.3.refs_4_
  66.5 1.9 %collective-permute-start.7 = (bf16[2048,128]{1,0:T(8,128)(2,1)S(1)}, bf16[2048,128]{1,0:T(8,128)(2,1)}, u32[]{:S(2)}, u32[]{:S(2)}) collective-permute-start(bf16[2048,128]{1,0:T(8,128)(2,1)S(1)} %collective-permute-done.3.refs_4_), channel_id=1, source_target_pairs={{0,64},{64,0},{128,192},{192,128},{256,320},{320,256},{384,448},{4... | collective-permute-start | bytes 1572872 | tf_op jit(solution)/shard_map/ppermute | solution.py:313
  68.5 0.0 collective-permute-done.2.refs_3_
  68.5 2.4 %collective-permute-start.6 = (bf16[2048,128]{1,0:T(8,128)(2,1)}, bf16[2048,128]{1,0:T(8,128)(2,1)}, u32[]{:S(2)}, u32[]{:S(2)}) collective-permute-start(bf16[2048,128]{1,0:T(8,128)(2,1)} %collective-permute-done.2.refs_3_), channel_id=1, source_target_pairs={{0,64},{64,0},{128,192},{192,128},{256,320},{320,256},{384,448},{4... | collective-permute-start | bytes 1572872 | tf_op jit(solution)/shard_map/ppermute | solution.py:313
  70.9 1.9 %collective-permute-start.5 = (bf16[2048,128]{1,0:T(8,128)(2,1)}, bf16[2048,128]{1,0:T(8,128)(2,1)}, u32[]{:S(2)}, u32[]{:S(2)}) collective-permute-start(bf16[2048,128]{1,0:T(8,128)(2,1)} %collective-permute-done.1.refs_2_), channel_id=1, source_target_pairs={{0,64},{64,0},{128,192},{192,128},{256,320},{320,256},{384,448},{4... | collective-permute-start | bytes 1572872 | tf_op jit(solution)/shard_map/ppermute | solution.py:313
  72.8 3.0 %inside.1 = (f32[256,1024]{1,0:T(8,128)S(1)}, bf16[256,512]{1,0:T(8,128)(2,1)S(1)}, f32[32,256]{1,0:T(8,128)S(1)}) custom-call(s32[3]{0:T(128)S(1)} %pad_add_fusion.who_ref, f32[256,512]{1,0:T(8,128)S(1)} %get-tuple-element.10.cum_ref, bf16[17,72,128]{2,1,0:T(8,128)(2,1)S(1)} %collective-permute-done.other_ref, bf16[256,512]{1,0:T(8,128)(2,1)} %bitcast.22, ...), custom_call_target="tpu_custom_call" | custom-call | flops 300000000 | bytes 1000000 | tf_op jit(solution)/shard_map/inside/pallas_call | solution.py:349
  75.8 0.0 all-to-all-done.got_ref
  75.9 0.2 chain.1
  76.1 19.1 %all_to_all.15.start_ref = bf16[16,32,256]{2,1,0:T(8,128)(2,1)S(1)} all-to-all(bf16[16,32,256]{2,1,0:T(8,128)(2,1)S(1)} %chain.1), channel_id=1, replica_groups=mesh['sp'=16,'dp'=64] {'sp'}, dimensions={0} | all-to-all | bytes 524288 | tf_op jit(solution)/shard_map/all_to_all | solution.py:379
  95.2 0.0 collective-permute-done.4.refs_5_
  95.2 0.0 collective-permute-done.7.refs_8_
  95.2 4.5 %project.1 = bf16[256,2048]{1,0:T(8,128)(2,1)} custom-call(s32[3]{0:T(128)S(1)} %pad_add_fusion.who_ref, f32[256,1024]{1,0:T(8,128)S(1)} %get-tuple-element.12.inside_ref, bf16[256,512]{1,0:T(8,128)(2,1)S(1)} %get-tuple-element.13.far_ref, bf16[16,32,256]{2,1,0:T(8,128)(2,1)S(1)} %all_to_all.15.start_ref, f32[1,256]{1,0:T(1,128)} %bitcast.24, ...), custom_call_target="tpu_custom_call" | custom-call | flops 1000000000 | bytes 1000000 | tf_op jit(solution)/shard_map/project/pallas_call | solution.py:381
  (8 shorter events, 0.0 us)
Async XLA Ops:
  2.3 41.4 %all-to-all-start.2 = ((bf16[64,32,128]{2,1,0:T(8,128)(2,1)}), bf16[64,32,128]{2,1,0:T(8,128)(2,1)S(1)}, u32[]{:S(2)}, u32[]{:S(2)}) async-start(bf16[64,32,128]{2,1,0:T(8,128)(2,1)} %spread.1), calls=%async_computation.2 | async-start | bytes 1048576 | tf_op jit(solution)/shard_map/all_to_all | solution.py:307
  29.0 23.5 %collective-permute-start = (bf16[17,72,128]{2,1,0:T(8,128)(2,1)S(1)}, bf16[17,72,128]{2,1,0:T(8,128)(2,1)S(1)}, u32[]{:S(2)}, u32[]{:S(2)}) collective-permute-start(bf16[17,72,128]{2,1,0:T(8,128)(2,1)S(1)} %get-tuple-element.11.own_ref), channel_id=1, source_target_pairs={{0,64},{64,0},{128,192},{192,128},{256,320},{320,256},{384,448},{4... | collective-permute-start | bytes 940040 | tf_op jit(solution)/shard_map/ppermute | solution.py:336
  43.7 16.8 %copy-start = (bf16[64,32,128]{2,1,0:T(8,128)(2,1)}, bf16[64,32,128]{2,1,0:T(8,128)(2,1)S(1)}, u32[]{:S(2)}) copy-start(bf16[64,32,128]{2,1,0:T(8,128)(2,1)S(1)} %all-to-all-done.2) | copy-start | bytes 1572868
  43.7 22.9 %collective-permute-start.3 = (bf16[2048,128]{1,0:T(8,128)(2,1)S(1)}, bf16[2048,128]{1,0:T(8,128)(2,1)S(1)}, u32[]{:S(2)}, u32[]{:S(2)}) collective-permute-start(bf16[2048,128]{1,0:T(8,128)(2,1)S(1)} %bitcast.12), channel_id=1, source_target_pairs={{7,0},{0,1},{1,2},{2,3},{3,4},{4,5},{5,6},{6,7},{15,8},{8,9},{9,10... | collective-permute-start | bytes 1572872 | tf_op jit(solution)/shard_map/ppermute | solution.py:310
  46.8 21.6 %collective-permute-start.2 = (bf16[2048,128]{1,0:T(8,128)(2,1)S(1)}, bf16[2048,128]{1,0:T(8,128)(2,1)}, u32[]{:S(2)}, u32[]{:S(2)}) collective-permute-start(bf16[2048,128]{1,0:T(8,128)(2,1)S(1)} %bitcast.13), channel_id=1, source_target_pairs={{8,0},{9,1},{10,2},{11,3},{12,4},{13,5},{14,6},{15,7},{16,8},{17,9... | collective-permute-start | bytes 1572872 | tf_op jit(solution)/shard_map/ppermute | solution.py:310
  49.3 21.5 %collective-permute-start.1 = (bf16[2048,128]{1,0:T(8,128)(2,1)S(1)}, bf16[2048,128]{1,0:T(8,128)(2,1)}, u32[]{:S(2)}, u32[]{:S(2)}) collective-permute-start(bf16[2048,128]{1,0:T(8,128)(2,1)S(1)} %bitcast.14), channel_id=1, source_target_pairs={{1,0},{2,1},{3,2},{4,3},{5,4},{6,5},{7,6},{0,7},{9,8},{10,9},{11,1... | collective-permute-start | bytes 1572872 | tf_op jit(solution)/shard_map/ppermute | solution.py:310
  54.0 21.9 %all-to-all-start = ((bf16[8,72,128]{2,1,0:T(8,128)(2,1)}), bf16[8,72,128]{2,1,0:T(8,128)(2,1)S(1)}, u32[]{:S(2)}, u32[]{:S(2)}) async-start(bf16[8,72,128]{2,1,0:T(8,128)(2,1)} %combine.1), calls=%async_computation | async-start | bytes 294912 | tf_op jit(solution)/shard_map/all_to_all | solution.py:347
  60.5 34.7 %collective-permute-start.4 = (bf16[2048,128]{1,0:T(8,128)(2,1)S(1)}, bf16[2048,128]{1,0:T(8,128)(2,1)}, u32[]{:S(2)}, u32[]{:S(2)}) collective-permute-start(bf16[2048,128]{1,0:T(8,128)(2,1)S(1)} %bitcast.15), channel_id=1, source_target_pairs={{0,64},{64,0},{128,192},{192,128},{256,320},{320,256},{384,448},{4... | collective-permute-start | bytes 1572872 | tf_op jit(solution)/shard_map/ppermute | solution.py:313
  66.5 9.3 %copy-start.1 = (bf16[2048,128]{1,0:T(8,128)(2,1)}, bf16[2048,128]{1,0:T(8,128)(2,1)S(1)}, u32[]{:S(2)}) copy-start(bf16[2048,128]{1,0:T(8,128)(2,1)S(1)} %collective-permute-done.3.refs_4_) | copy-start | bytes 1572868
  66.5 28.6 %collective-permute-start.7 = (bf16[2048,128]{1,0:T(8,128)(2,1)S(1)}, bf16[2048,128]{1,0:T(8,128)(2,1)}, u32[]{:S(2)}, u32[]{:S(2)}) collective-permute-start(bf16[2048,128]{1,0:T(8,128)(2,1)S(1)} %collective-permute-done.3.refs_4_), channel_id=1, source_target_pairs={{0,64},{64,0},{128,192},{192,128},{256,320},{320,256},{384,448},{4... | collective-permute-start | bytes 1572872 | tf_op jit(solution)/shard_map/ppermute | solution.py:313
  68.5 26.7 %collective-permute-start.6 = (bf16[2048,128]{1,0:T(8,128)(2,1)}, bf16[2048,128]{1,0:T(8,128)(2,1)}, u32[]{:S(2)}, u32[]{:S(2)}) collective-permute-start(bf16[2048,128]{1,0:T(8,128)(2,1)} %collective-permute-done.2.refs_3_), channel_id=1, source_target_pairs={{0,64},{64,0},{128,192},{192,128},{256,320},{320,256},{384,448},{4... | collective-permute-start | bytes 1572872 | tf_op jit(solution)/shard_map/ppermute | solution.py:313
  70.9 24.3 %collective-permute-start.5 = (bf16[2048,128]{1,0:T(8,128)(2,1)}, bf16[2048,128]{1,0:T(8,128)(2,1)}, u32[]{:S(2)}, u32[]{:S(2)}) collective-permute-start(bf16[2048,128]{1,0:T(8,128)(2,1)} %collective-permute-done.1.refs_2_), channel_id=1, source_target_pairs={{0,64},{64,0},{128,192},{192,128},{256,320},{320,256},{384,448},{4... | collective-permute-start | bytes 1572872 | tf_op jit(solution)/shard_map/ppermute | solution.py:313

commit v5 on v4

--- a/solution.py
+++ b/solution.py
@@ -68,17 +68,21 @@
     return copies
 
 
-def spread_kernel(who_ref, weight_hbm, out_ref, quarters, sems):
+def spread_kernel(who_ref, weight_hbm, out_hbm, quarters, pattern, sems, out_sems):
     core = who_ref[1]
-    width = out_ref.shape[2]
+    width = quarters.shape[2]
     pairs = []
     for c in range(4):
         first = pl.multiple_of((core * 4 + c) * width, width)
         pairs.append((weight_hbm.at[:, pl.ds(first, width)], quarters.at[c]))
     for c in fetch(sems, *pairs):
         c.wait()
-    for d in range(out_ref.shape[0]):
-        out_ref[d] = quarters[(d % SIDE + 2 * (d // SIDE)) % 4]
+    period = pattern.shape[0]
+    for d in range(period):
+        pattern[d] = quarters[(d % SIDE + 2 * (d // SIDE)) % 4]
+    spans = range(0, out_hbm.shape[0], period)
+    for c in fetch(out_sems, *[(pattern, out_hbm.at[pl.ds(d, period)]) for d in spans]):
+        c.wait()
 
 
 def summary_kernel(k_hbm, x_hbm, v_hbm, extra_hbm, bias_hbm, send_ref, cum_ref, k_ref, x_ref, v_ref, extra_ref, bias_ref, sems):
@@ -296,10 +300,15 @@
 
     spread = pl.pallas_call(
         spread_kernel,
-        out_shape=pltpu.VMEM((plane, share, piece), BF16),
+        out_shape=pltpu.HBM((plane, share, piece), BF16),
         in_specs=[SMEM, HBM],
-        out_specs=VMEM,
-        scratch_shapes=[pltpu.VMEM((4, share, piece), BF16), dma((4,))],
+        out_specs=HBM,
+        scratch_shapes=[
+            pltpu.VMEM((4, share, piece), BF16),
+            pltpu.VMEM((2 * SIDE, share, piece), BF16),
+            dma((4,)),
+            dma((plane // (2 * SIDE),)),
+        ],
         compiler_params=params(4),
         cost_estimate=cost(10**6),
         name="spread",

time: 100 us -> 100 us (level)
  no operation moved by 1% of the time
where the time goes in v5:
time: 100 us; the launch traced here: 99.6 us
  starting transfers between devices  54.5 us (54%)
  blocking collectives  19.1 us (19%)
  Pallas kernels  14 us (14%)
  waiting for transfers between devices  11.8 us (12%)
    all_to_all x1, starting transfers between devices, on_device(): lax.all_to_all(spread, 'dp', 0, 0, tiled=True).reshape(model, piece)  24 us
    all_to_all x1, blocking collectives, on_device(): start = lax.all_to_all(starts, 'sp', 0, 0, tiled=True)  19.1 us
    ppermute x4, starting transfers between devices, on_device(): other.append(lax.ppermute(chunk, 'sp', [(i, i ^ 1) for i in range(group)]))  12.3 us
    all_to_all x1, waiting for transfers between devices, on_device(): lax.all_to_all(spread, 'dp', 0, 0, tiled=True).reshape(model, piece)  11.8 us
    ppermute x3, starting transfers between devices, on_device(): mine.append(lax.ppermute(eighth, 'dp', from_offset(*o)))  8.85 us
    all_to_all x1, starting transfers between devices, on_device(): got = lax.all_to_all(send, 'sp', 0, 0, axis_index_groups=chips, tiled=True)  6.48 us
    pallas_call x1, Pallas kernels, on_device(): pl.pallas_call(project_kernel, out_shape=jax.ShapeDtypeStruct((tok, model...  4.46 us
    pallas_call x1, Pallas kernels, on_device(): pl.pallas_call(inside_kernel, out_shape=(pltpu.VMEM((tok, heads * vd), F3...  3.01 us
  transfers between devices with their start and end apart: 10, of which 1 were waited for; matrix products, arithmetic and copies ran while one was open for 0% of the time, Pallas kernels for 7%

profile of v5, /device:TPU:1, one launch (start us, length us, event | category | flops | bytes accessed | tf_op | source)
XLA Modules:
  0.0 99.6 jit_solution(7353576735448688244)
XLA Ops:
  0.0 0.1 pad_add_fusion.who_ref
  0.1 2.2 %spread.1 = bf16[64,32,128]{2,1,0:T(8,128)(2,1)} custom-call(s32[3]{0:T(128)S(1)} %pad_add_fusion.who_ref, bf16[32,1024]{1,0:T(8,128)(2,1)} %bitcast.23), custom_call_target="tpu_custom_call" | custom-call | flops 1000000 | bytes 1000000 | tf_op jit(solution)/shard_map/spread/pallas_call | solution.py:301
  2.2 24.0 %all-to-all-start.2 = ((bf16[64,32,128]{2,1,0:T(8,128)(2,1)}), bf16[64,32,128]{2,1,0:T(8,128)(2,1)S(1)}, u32[]{:S(2)}, u32[]{:S(2)}) async-start(bf16[64,32,128]{2,1,0:T(8,128)(2,1)} %spread.1), calls=%async_computation.2 | async-start | bytes 1048576 | tf_op jit(solution)/shard_map/all_to_all | solution.py:316
  26.2 2.8 %summary.1 = (bf16[17,72,128]{2,1,0:T(8,128)(2,1)S(1)}, f32[256,512]{1,0:T(8,128)S(1)}) custom-call(bf16[256,512]{1,0:T(8,128)(2,1)} %bitcast.20, bf16[256,512]{1,0:T(8,128)(2,1)} %bitcast.25, bf16[256,1024]{1,0:T(8,128)(2,1)} %bitcast.17, f32[4,256]{1,0:T(4,128)} %extra_hbm.1, f32[4,128]{1,0:T(4,128)} %bias_hbm.1), custom_call_target="tpu_custom_call" | custom-call | flops 300000000 | bytes 1000000 | tf_op jit(solution)/shard_map/summary/pallas_call | solution.py:324
  29.0 2.9 %collective-permute-start = (bf16[17,72,128]{2,1,0:T(8,128)(2,1)S(1)}, bf16[17,72,128]{2,1,0:T(8,128)(2,1)S(1)}, u32[]{:S(2)}, u32[]{:S(2)}) collective-permute-start(bf16[17,72,128]{2,1,0:T(8,128)(2,1)S(1)} %get-tuple-element.11.own_ref), channel_id=1, source_target_pairs={{0,64},{64,0},{128,192},{192,128},{256,320},{320,256},{384,448},{4... | collective-permute-start | bytes 940040 | tf_op jit(solution)/shard_map/ppermute | solution.py:345
  31.9 11.8 %all-to-all-done.2 = bf16[64,32,128]{2,1,0:T(8,128)(2,1)S(1)} async-done(((bf16[64,32,128]{2,1,0:T(8,128)(2,1)}), bf16[64,32,128]{2,1,0:T(8,128)(2,1)S(1)}, u32[]{:S(2)}, u32[]{:S(2)}) %all-to-all-start.2) | async-done | bytes 524320 | tf_op jit(solution)/shard_map/all_to_all | solution.py:316
  43.6 3.2 %collective-permute-start.3 = (bf16[2048,128]{1,0:T(8,128)(2,1)S(1)}, bf16[2048,128]{1,0:T(8,128)(2,1)S(1)}, u32[]{:S(2)}, u32[]{:S(2)}) collective-permute-start(bf16[2048,128]{1,0:T(8,128)(2,1)S(1)} %bitcast.12), channel_id=1, source_target_pairs={{7,0},{0,1},{1,2},{2,3},{3,4},{4,5},{5,6},{6,7},{15,8},{8,9},{9,10... | collective-permute-start | bytes 1572872 | tf_op jit(solution)/shard_map/ppermute | solution.py:319
  46.8 2.5 %collective-permute-start.2 = (bf16[2048,128]{1,0:T(8,128)(2,1)S(1)}, bf16[2048,128]{1,0:T(8,128)(2,1)}, u32[]{:S(2)}, u32[]{:S(2)}) collective-permute-start(bf16[2048,128]{1,0:T(8,128)(2,1)S(1)} %bitcast.13), channel_id=1, source_target_pairs={{8,0},{9,1},{10,2},{11,3},{12,4},{13,5},{14,6},{15,7},{16,8},{17,9... | collective-permute-start | bytes 1572872 | tf_op jit(solution)/shard_map/ppermute | solution.py:319
  49.3 3.2 %collective-permute-start.1 = (bf16[2048,128]{1,0:T(8,128)(2,1)S(1)}, bf16[2048,128]{1,0:T(8,128)(2,1)}, u32[]{:S(2)}, u32[]{:S(2)}) collective-permute-start(bf16[2048,128]{1,0:T(8,128)(2,1)S(1)} %bitcast.14), channel_id=1, source_target_pairs={{1,0},{2,1},{3,2},{4,3},{5,4},{6,5},{7,6},{0,7},{9,8},{10,9},{11,1... | collective-permute-start | bytes 1572872 | tf_op jit(solution)/shard_map/ppermute | solution.py:319
  52.5 0.0 collective-permute-done.other_ref
  52.5 1.4 %combine.1 = bf16[8,72,128]{2,1,0:T(8,128)(2,1)} custom-call(s32[3]{0:T(128)S(1)} %pad_add_fusion.who_ref, bf16[17,72,128]{2,1,0:T(8,128)(2,1)S(1)} %get-tuple-element.11.own_ref, bf16[17,72,128]{2,1,0:T(8,128)(2,1)S(1)} %collective-permute-done.other_ref), custom_call_target="tpu_custom_call" | custom-call | flops 10000000 | bytes 1000000 | tf_op jit(solution)/shard_map/combine/pallas_call | solution.py:346
  53.9 6.5 %all-to-all-start = ((bf16[8,72,128]{2,1,0:T(8,128)(2,1)}), bf16[8,72,128]{2,1,0:T(8,128)(2,1)S(1)}, u32[]{:S(2)}, u32[]{:S(2)}) async-start(bf16[8,72,128]{2,1,0:T(8,128)(2,1)} %combine.1), calls=%async_computation | async-start | bytes 294912 | tf_op jit(solution)/shard_map/all_to_all | solution.py:356
  60.4 6.0 %collective-permute-start.4 = (bf16[2048,128]{1,0:T(8,128)(2,1)S(1)}, bf16[2048,128]{1,0:T(8,128)(2,1)}, u32[]{:S(2)}, u32[]{:S(2)}) collective-permute-start(bf16[2048,128]{1,0:T(8,128)(2,1)S(1)} %bitcast.15), channel_id=1, source_target_pairs={{0,64},{64,0},{128,192},{192,128},{256,320},{320,256},{384,448},{4... | collective-permute-start | bytes 1572872 | tf_op jit(solution)/shard_map/ppermute | solution.py:322
  66.5 0.0 collective-permute-done.3.refs_4_
  66.5 1.9 %collective-permute-start.7 = (bf16[2048,128]{1,0:T(8,128)(2,1)S(1)}, bf16[2048,128]{1,0:T(8,128)(2,1)}, u32[]{:S(2)}, u32[]{:S(2)}) collective-permute-start(bf16[2048,128]{1,0:T(8,128)(2,1)S(1)} %collective-permute-done.3.refs_4_), channel_id=1, source_target_pairs={{0,64},{64,0},{128,192},{192,128},{256,320},{320,256},{384,448},{4... | collective-permute-start | bytes 1572872 | tf_op jit(solution)/shard_map/ppermute | solution.py:322
  68.4 0.0 collective-permute-done.2.refs_3_
  68.4 2.4 %collective-permute-start.6 = (bf16[2048,128]{1,0:T(8,128)(2,1)}, bf16[2048,128]{1,0:T(8,128)(2,1)}, u32[]{:S(2)}, u32[]{:S(2)}) collective-permute-start(bf16[2048,128]{1,0:T(8,128)(2,1)} %collective-permute-done.2.refs_3_), channel_id=1, source_target_pairs={{0,64},{64,0},{128,192},{192,128},{256,320},{320,256},{384,448},{4... | collective-permute-start | bytes 1572872 | tf_op jit(solution)/shard_map/ppermute | solution.py:322
  70.9 0.0 collective-permute-done.1.refs_2_
  70.9 1.9 %collective-permute-start.5 = (bf16[2048,128]{1,0:T(8,128)(2,1)}, bf16[2048,128]{1,0:T(8,128)(2,1)}, u32[]{:S(2)}, u32[]{:S(2)}) collective-permute-start(bf16[2048,128]{1,0:T(8,128)(2,1)} %collective-permute-done.1.refs_2_), channel_id=1, source_target_pairs={{0,64},{64,0},{128,192},{192,128},{256,320},{320,256},{384,448},{4... | collective-permute-start | bytes 1572872 | tf_op jit(solution)/shard_map/ppermute | solution.py:322
  72.8 3.0 %inside.1 = (f32[256,1024]{1,0:T(8,128)S(1)}, bf16[256,512]{1,0:T(8,128)(2,1)S(1)}, f32[32,256]{1,0:T(8,128)S(1)}) custom-call(s32[3]{0:T(128)S(1)} %pad_add_fusion.who_ref, f32[256,512]{1,0:T(8,128)S(1)} %get-tuple-element.10.cum_ref, bf16[17,72,128]{2,1,0:T(8,128)(2,1)S(1)} %collective-permute-done.other_ref, bf16[256,512]{1,0:T(8,128)(2,1)} %bitcast.22, ...), custom_call_target="tpu_custom_call" | custom-call | flops 300000000 | bytes 1000000 | tf_op jit(solution)/shard_map/inside/pallas_call | solution.py:358
  75.8 0.2 chain.1
  76.0 19.1 %all_to_all.15.start_ref = bf16[16,32,256]{2,1,0:T(8,128)(2,1)S(1)} all-to-all(bf16[16,32,256]{2,1,0:T(8,128)(2,1)S(1)} %chain.1), channel_id=1, replica_groups=mesh['sp'=16,'dp'=64] {'sp'}, dimensions={0} | all-to-all | bytes 524288 | tf_op jit(solution)/shard_map/all_to_all | solution.py:388
  95.1 0.0 collective-permute-done.5.refs_6_
  95.1 4.5 %project.1 = bf16[256,2048]{1,0:T(8,128)(2,1)} custom-call(s32[3]{0:T(128)S(1)} %pad_add_fusion.who_ref, f32[256,1024]{1,0:T(8,128)S(1)} %get-tuple-element.12.inside_ref, bf16[256,512]{1,0:T(8,128)(2,1)S(1)} %get-tuple-element.13.far_ref, bf16[16,32,256]{2,1,0:T(8,128)(2,1)S(1)} %all_to_all.15.start_ref, f32[1,256]{1,0:T(1,128)} %bitcast.24, ...), custom_call_target="tpu_custom_call" | custom-call | flops 1000000000 | bytes 1000000 | tf_op jit(solution)/shard_map/project/pallas_call | solution.py:390
  (8 shorter events, 0.0 us)
Async XLA Ops:
  2.2 41.4 %all-to-all-start.2 = ((bf16[64,32,128]{2,1,0:T(8,128)(2,1)}), bf16[64,32,128]{2,1,0:T(8,128)(2,1)S(1)}, u32[]{:S(2)}, u32[]{:S(2)}) async-start(bf16[64,32,128]{2,1,0:T(8,128)(2,1)} %spread.1), calls=%async_computation.2 | async-start | bytes 1048576 | tf_op jit(solution)/shard_map/all_to_all | solution.py:316
  29.0 23.5 %collective-permute-start = (bf16[17,72,128]{2,1,0:T(8,128)(2,1)S(1)}, bf16[17,72,128]{2,1,0:T(8,128)(2,1)S(1)}, u32[]{:S(2)}, u32[]{:S(2)}) collective-permute-start(bf16[17,72,128]{2,1,0:T(8,128)(2,1)S(1)} %get-tuple-element.11.own_ref), channel_id=1, source_target_pairs={{0,64},{64,0},{128,192},{192,128},{256,320},{320,256},{384,448},{4... | collective-permute-start | bytes 940040 | tf_op jit(solution)/shard_map/ppermute | solution.py:345
  43.6 16.8 %copy-start = (bf16[64,32,128]{2,1,0:T(8,128)(2,1)}, bf16[64,32,128]{2,1,0:T(8,128)(2,1)S(1)}, u32[]{:S(2)}) copy-start(bf16[64,32,128]{2,1,0:T(8,128)(2,1)S(1)} %all-to-all-done.2) | copy-start | bytes 1572868
  43.6 22.9 %collective-permute-start.3 = (bf16[2048,128]{1,0:T(8,128)(2,1)S(1)}, bf16[2048,128]{1,0:T(8,128)(2,1)S(1)}, u32[]{:S(2)}, u32[]{:S(2)}) collective-permute-start(bf16[2048,128]{1,0:T(8,128)(2,1)S(1)} %bitcast.12), channel_id=1, source_target_pairs={{7,0},{0,1},{1,2},{2,3},{3,4},{4,5},{5,6},{6,7},{15,8},{8,9},{9,10... | collective-permute-start | bytes 1572872 | tf_op jit(solution)/shard_map/ppermute | solution.py:319
  46.8 21.6 %collective-permute-start.2 = (bf16[2048,128]{1,0:T(8,128)(2,1)S(1)}, bf16[2048,128]{1,0:T(8,128)(2,1)}, u32[]{:S(2)}, u32[]{:S(2)}) collective-permute-start(bf16[2048,128]{1,0:T(8,128)(2,1)S(1)} %bitcast.13), channel_id=1, source_target_pairs={{8,0},{9,1},{10,2},{11,3},{12,4},{13,5},{14,6},{15,7},{16,8},{17,9... | collective-permute-start | bytes 1572872 | tf_op jit(solution)/shard_map/ppermute | solution.py:319
  49.3 21.5 %collective-permute-start.1 = (bf16[2048,128]{1,0:T(8,128)(2,1)S(1)}, bf16[2048,128]{1,0:T(8,128)(2,1)}, u32[]{:S(2)}, u32[]{:S(2)}) collective-permute-start(bf16[2048,128]{1,0:T(8,128)(2,1)S(1)} %bitcast.14), channel_id=1, source_target_pairs={{1,0},{2,1},{3,2},{4,3},{5,4},{6,5},{7,6},{0,7},{9,8},{10,9},{11,1... | collective-permute-start | bytes 1572872 | tf_op jit(solution)/shard_map/ppermute | solution.py:319
  53.9 21.9 %all-to-all-start = ((bf16[8,72,128]{2,1,0:T(8,128)(2,1)}), bf16[8,72,128]{2,1,0:T(8,128)(2,1)S(1)}, u32[]{:S(2)}, u32[]{:S(2)}) async-start(bf16[8,72,128]{2,1,0:T(8,128)(2,1)} %combine.1), calls=%async_computation | async-start | bytes 294912 | tf_op jit(solution)/shard_map/all_to_all | solution.py:356
  60.4 34.7 %collective-permute-start.4 = (bf16[2048,128]{1,0:T(8,128)(2,1)S(1)}, bf16[2048,128]{1,0:T(8,128)(2,1)}, u32[]{:S(2)}, u32[]{:S(2)}) collective-permute-start(bf16[2048,128]{1,0:T(8,128)(2,1)S(1)} %bitcast.15), channel_id=1, source_target_pairs={{0,64},{64,0},{128,192},{192,128},{256,320},{320,256},{384,448},{4... | collective-permute-start | bytes 1572872 | tf_op jit(solution)/shard_map/ppermute | solution.py:322
  66.5 9.3 %copy-start.1 = (bf16[2048,128]{1,0:T(8,128)(2,1)}, bf16[2048,128]{1,0:T(8,128)(2,1)S(1)}, u32[]{:S(2)}) copy-start(bf16[2048,128]{1,0:T(8,128)(2,1)S(1)} %collective-permute-done.3.refs_4_) | copy-start | bytes 1572868
  66.5 28.6 %collective-permute-start.7 = (bf16[2048,128]{1,0:T(8,128)(2,1)S(1)}, bf16[2048,128]{1,0:T(8,128)(2,1)}, u32[]{:S(2)}, u32[]{:S(2)}) collective-permute-start(bf16[2048,128]{1,0:T(8,128)(2,1)S(1)} %collective-permute-done.3.refs_4_), channel_id=1, source_target_pairs={{0,64},{64,0},{128,192},{192,128},{256,320},{320,256},{384,448},{4... | collective-permute-start | bytes 1572872 | tf_op jit(solution)/shard_map/ppermute | solution.py:322
  68.4 26.7 %collective-permute-start.6 = (bf16[2048,128]{1,0:T(8,128)(2,1)}, bf16[2048,128]{1,0:T(8,128)(2,1)}, u32[]{:S(2)}, u32[]{:S(2)}) collective-permute-start(bf16[2048,128]{1,0:T(8,128)(2,1)} %collective-permute-done.2.refs_3_), channel_id=1, source_target_pairs={{0,64},{64,0},{128,192},{192,128},{256,320},{320,256},{384,448},{4... | collective-permute-start | bytes 1572872 | tf_op jit(solution)/shard_map/ppermute | solution.py:322
  70.9 24.3 %collective-permute-start.5 = (bf16[2048,128]{1,0:T(8,128)(2,1)}, bf16[2048,128]{1,0:T(8,128)(2,1)}, u32[]{:S(2)}, u32[]{:S(2)}) collective-permute-start(bf16[2048,128]{1,0:T(8,128)(2,1)} %collective-permute-done.1.refs_2_), channel_id=1, source_target_pairs={{0,64},{64,0},{128,192},{192,128},{256,320},{320,256},{384,448},{4... | collective-permute-start | bytes 1572872 | tf_op jit(solution)/shard_map/ppermute | solution.py:322

commit v6 on v3

--- a/solution.py
+++ b/solution.py
@@ -13,7 +13,6 @@
 BF16 = jnp.bfloat16
 VMEM = pl.BlockSpec(memory_space=pltpu.VMEM)
 HBM = pl.BlockSpec(memory_space=pltpu.HBM)
-SMEM = pl.BlockSpec(memory_space=pltpu.SMEM)
 SIDE = 8
 TILES = 4
 
@@ -33,17 +32,27 @@
     return copies
 
 
-def spread_kernel(who_ref, weight_hbm, out_ref, quarters, sems):
-    core = who_ref[1]
-    width = out_ref.shape[2]
+def place():
+    sp, dp = lax.axis_index("sp"), lax.axis_index("dp")
+    color = lax.rem(lax.rem(dp, SIDE) + 2 * lax.div(dp, SIDE), 4)
+    return sp, lax.rem(sp, 2), color
+
+
+def spread_kernel(weight_hbm, out_hbm, quarters, pattern, sems, out_sems):
+    _, core, _ = place()
+    width = quarters.shape[2]
     pairs = []
     for c in range(4):
         first = pl.multiple_of((core * 4 + c) * width, width)
         pairs.append((weight_hbm.at[:, pl.ds(first, width)], quarters.at[c]))
     for c in fetch(sems, *pairs):
         c.wait()
-    for d in range(out_ref.shape[0]):
-        out_ref[d] = quarters[(d % SIDE + 2 * (d // SIDE)) % 4]
+    period = pattern.shape[0]
+    for d in range(period):
+        pattern[d] = quarters[(d % SIDE + 2 * (d // SIDE)) % 4]
+    spans = range(0, out_hbm.shape[0], period)
+    for c in fetch(out_sems, *[(pattern, out_hbm.at[pl.ds(d, period)]) for d in spans]):
+        c.wait()
 
 
 def summary_kernel(k_hbm, x_hbm, v_hbm, extra_hbm, bias_hbm, send_ref, cum_ref, k_ref, x_ref, v_ref, extra_ref, bias_ref, sems):
@@ -95,10 +104,10 @@
 
 
 def inside_kernel(
-    who_ref, cum_ref, q_hbm, k_hbm, v_hbm, open_hbm, inside_ref, far_ref, open_ref, q_ref, k_ref, v_ref, sems
+    cum_ref, q_hbm, k_hbm, v_hbm, open_hbm, inside_ref, far_ref, open_ref, q_ref, k_ref, v_ref, sems
 ):
     mine = open_ref.shape[0]
-    first = pl.multiple_of(who_ref[0] * mine, mine)
+    first = pl.multiple_of(place()[0] * mine, mine)
     for c in fetch(
         sems, (q_hbm, q_ref), (k_hbm, k_ref), (v_hbm, v_ref), (open_hbm.at[pl.ds(first, mine), :], open_ref)
     ):
@@ -153,10 +162,10 @@
             states[w] = rate * states[w] + got_ref[d, w * rows : (w + 1) * rows, :].astype(F32)
 
 
-def project_kernel(who_ref, inside_ref, far_ref, start_ref, *refs):
+def project_kernel(inside_ref, far_ref, start_ref, *refs):
     gain_hbm, mine, other, out_hbm = refs[0], refs[1:5], refs[5:9], refs[9]
     normed, weight, gain_ref, tiles, in_sems, out_sems = refs[10:]
-    core, color = who_ref[1], who_ref[2]
+    _, core, color = place()
     half = normed.shape[1] // 2
     piece = half // 4
     model = weight.shape[0]
@@ -232,9 +241,6 @@
     piece = heads * vd // 8
     rows = heads * kd // group
     packed = rows * vd // 128 + 8
-    sp, dp = lax.axis_index("sp"), lax.axis_index("dp")
-    z, y = lax.div(dp, SIDE), lax.rem(dp, SIDE)
-    who = jnp.stack([sp, lax.rem(sp, 2), lax.rem(y + 2 * z, 4), z]).astype(jnp.int32)
     dma = pltpu.SemaphoreType.DMA
 
     q = queries.reshape(tok, width)
@@ -252,14 +258,19 @@
 
     spread = pl.pallas_call(
         spread_kernel,
-        out_shape=pltpu.VMEM((plane, share, piece), BF16),
-        in_specs=[SMEM, HBM],
-        out_specs=VMEM,
-        scratch_shapes=[pltpu.VMEM((4, share, piece), BF16), dma((4,))],
+        out_shape=pltpu.HBM((plane, share, piece), BF16),
+        in_specs=[HBM],
+        out_specs=HBM,
+        scratch_shapes=[
+            pltpu.VMEM((4, share, piece), BF16),
+            pltpu.VMEM((2 * SIDE, share, piece), BF16),
+            dma((4,)),
+            dma((plane // (2 * SIDE),)),
+        ],
         compiler_params=params(4),
         cost_estimate=cost(10**6),
         name="spread",
-    )(who, *hbm(output_weight.T))
+    )(*hbm(output_weight.T))
     eighth = lax.all_to_all(spread, "dp", 0, 0, tiled=True).reshape(model, piece)
     mine = [eighth]
     for o in ((0, 1), (1, 0), (0, -1)):
@@ -298,7 +309,7 @@
             pltpu.VMEM((tok, width), BF16),
             pltpu.VMEM((rows, vd), F32),
         ),
-        in_specs=[SMEM, VMEM] + [HBM] * 4,
+        in_specs=[VMEM] + [HBM] * 4,
         out_specs=(VMEM, VMEM, VMEM),
         scratch_shapes=[
             pltpu.VMEM((tok, width), BF16),
@@ -309,7 +320,7 @@
         compiler_params=params(16),
         cost_estimate=cost(3 * 10**8),
         name="inside",
-    )(who, *vmem(cum), *hbm(q, k, v, opening))
+    )(*vmem(cum), *hbm(q, k, v, opening))
 
     starts = pl.pallas_call(
         chain_kernel,
@@ -326,7 +337,7 @@
     out = pl.pallas_call(
         project_kernel,
         out_shape=jax.ShapeDtypeStruct((tok, model), BF16),
-        in_specs=[SMEM] + [VMEM] * 3 + [HBM] * 9,
+        in_specs=[VMEM] * 3 + [HBM] * 9,
         out_specs=HBM,
         scratch_shapes=[
             pltpu.VMEM((tok, heads * vd), BF16),
@@ -339,7 +350,7 @@
         compiler_params=params(24),
         cost_estimate=cost(10**9),
         name="project",
-    )(who, *vmem(inside, far, start), *hbm(output_norm_gain.reshape(1, vd), *mine, *other))
+    )(*vmem(inside, far, start), *hbm(output_norm_gain.reshape(1, vd), *mine, *other))
     return out.reshape(tok, seqs, model)
 
 

time: 102 us -> 101 us (level)
  transfers between devices with their start and end apart: 8 -> 8, of which waited for: 0 -> 1; matrix products, arithmetic and copies ran while one was open for 0% -> 0% of each run, Pallas kernels for 7% -> 7%
where the time goes in v6:
time: 101 us
  blocking collectives  59.7 us (59%)
  starting transfers between devices  28.2 us (28%)
  Pallas kernels  12.6 us (12%)
    all_to_all x1, blocking collectives, on_device(): lax.all_to_all(spread, 'dp', 0, 0, tiled=True).reshape(model, piece)  41.4 us
    all_to_all x1, blocking collectives, on_device(): lax.all_to_all(starts, 'sp', 0, 0, tiled=True).reshape(heads * kd, vd)  18.4 us
    all_to_all x1, starting transfers between devices, on_device(): got = lax.all_to_all(send, 'sp', 0, 0, tiled=True)  10.6 us
    ppermute x3, starting transfers between devices, on_device(): mine.append(lax.ppermute(eighth, 'dp', from_offset(*o)))  8.85 us
    ppermute x4, starting transfers between devices, on_device(): other.append(lax.ppermute(chunk, 'sp', [(i, i ^ 1) for i in range(group)]))  8.66 us
    pallas_call x1, Pallas kernels, on_device(): pl.pallas_call(project_kernel, out_shape=jax.ShapeDtypeStruct((tok, model...  3.92 us
    pallas_call x1, Pallas kernels, on_device(): pl.pallas_call(summary_kernel, out_shape=(pltpu.VMEM((group, packed, 128)...  3.5 us
    pallas_call x1, Pallas kernels, on_device(): pl.pallas_call(inside_kernel, out_shape=(pltpu.VMEM((tok, heads * vd), F3...  3.29 us
  transfers between devices with their start and end apart: 8, of which 1 were waited for; matrix products, arithmetic and copies ran while one was open for 0% of the time, Pallas kernels for 7%

profile of v6, /device:TPU:1, one launch (start us, length us, event | category | flops | bytes accessed | tf_op | source)
XLA Modules:
  0.0 100.9 jit_solution(6565354692765102208)
XLA Ops:
  0.0 1.6 %spread.1 = bf16[64,32,128]{2,1,0:T(8,128)(2,1)} custom-call(bf16[32,1024]{1,0:T(8,128)(2,1)} %bitcast.22), custom_call_target="tpu_custom_call" | custom-call | flops 1000000 | bytes 1000000 | tf_op jit(solution)/shard_map/spread/pallas_call | solution.py:259
  1.6 41.4 %all_to_all.15 = bf16[64,32,128]{2,1,0:T(8,128)(2,1)S(1)} all-to-all(bf16[64,32,128]{2,1,0:T(8,128)(2,1)} %spread.1), channel_id=1, replica_groups=mesh['sp'=16,'dp'=64] {'dp'}, dimensions={0} | all-to-all | bytes 1048576 | tf_op jit(solution)/shard_map/all_to_all | solution.py:274
  43.0 3.2 %collective-permute-start.2 = (bf16[2048,128]{1,0:T(8,128)(2,1)S(1)}, bf16[2048,128]{1,0:T(8,128)(2,1)S(1)}, u32[]{:S(2)}, u32[]{:S(2)}) collective-permute-start(bf16[2048,128]{1,0:T(8,128)(2,1)S(1)} %bitcast.11), channel_id=1, source_target_pairs={{7,0},{0,1},{1,2},{2,3},{3,4},{4,5},{5,6},{6,7},{15,8},{8,9},{9,10... | collective-permute-start | bytes 1572872 | tf_op jit(solution)/shard_map/ppermute | solution.py:277
  46.2 2.5 %collective-permute-start.1 = (bf16[2048,128]{1,0:T(8,128)(2,1)S(1)}, bf16[2048,128]{1,0:T(8,128)(2,1)}, u32[]{:S(2)}, u32[]{:S(2)}) collective-permute-start(bf16[2048,128]{1,0:T(8,128)(2,1)S(1)} %bitcast.12), channel_id=1, source_target_pairs={{8,0},{9,1},{10,2},{11,3},{12,4},{13,5},{14,6},{15,7},{16,8},{17,9... | collective-permute-start | bytes 1572872 | tf_op jit(solution)/shard_map/ppermute | solution.py:277
  48.7 3.2 %collective-permute-start = (bf16[2048,128]{1,0:T(8,128)(2,1)S(1)}, bf16[2048,128]{1,0:T(8,128)(2,1)}, u32[]{:S(2)}, u32[]{:S(2)}) collective-permute-start(bf16[2048,128]{1,0:T(8,128)(2,1)S(1)} %bitcast.13), channel_id=1, source_target_pairs={{1,0},{2,1},{3,2},{4,3},{5,4},{6,5},{7,6},{0,7},{9,8},{10,9},{11,1... | collective-permute-start | bytes 1572872 | tf_op jit(solution)/shard_map/ppermute | solution.py:277
  51.9 3.5 %summary.1 = (bf16[16,72,128]{2,1,0:T(8,128)(2,1)}, f32[256,512]{1,0:T(8,128)S(1)}) custom-call(bf16[256,512]{1,0:T(8,128)(2,1)} %bitcast.19, bf16[256,512]{1,0:T(8,128)(2,1)} %bitcast.24, bf16[256,1024]{1,0:T(8,128)(2,1)} %bitcast.16, f32[4,256]{1,0:T(4,128)} %extra_hbm.1, f32[4,128]{1,0:T(4,128)} %bias_hbm.1), custom_call_target="tpu_custom_call" | custom-call | flops 300000000 | bytes 1000000 | tf_op jit(solution)/shard_map/summary/pallas_call | solution.py:282
  55.4 10.6 %all-to-all-start = ((bf16[16,72,128]{2,1,0:T(8,128)(2,1)}), bf16[16,72,128]{2,1,0:T(8,128)(2,1)S(1)}, u32[]{:S(2)}, u32[]{:S(2)}) async-start(bf16[16,72,128]{2,1,0:T(8,128)(2,1)} %get-tuple-element.13), calls=%async_computation | async-start | bytes 589824 | tf_op jit(solution)/shard_map/all_to_all | solution.py:303
  66.0 0.0 copy-done
  66.0 2.0 %collective-permute-start.3 = (bf16[2048,128]{1,0:T(8,128)(2,1)S(1)}, bf16[2048,128]{1,0:T(8,128)(2,1)}, u32[]{:S(2)}, u32[]{:S(2)}) collective-permute-start(bf16[2048,128]{1,0:T(8,128)(2,1)S(1)} %bitcast.14), channel_id=1, source_target_pairs={{0,64},{64,0},{128,192},{192,128},{256,320},{320,256},{384,448},{4... | collective-permute-start | bytes 1572872 | tf_op jit(solution)/shard_map/ppermute | solution.py:280
  68.1 0.0 collective-permute-done.2.refs_4_
  68.1 2.3 %collective-permute-start.6 = (bf16[2048,128]{1,0:T(8,128)(2,1)S(1)}, bf16[2048,128]{1,0:T(8,128)(2,1)}, u32[]{:S(2)}, u32[]{:S(2)}) collective-permute-start(bf16[2048,128]{1,0:T(8,128)(2,1)S(1)} %collective-permute-done.2.refs_4_), channel_id=1, source_target_pairs={{0,64},{64,0},{128,192},{192,128},{256,320},{320,256},{384,448},{4... | collective-permute-start | bytes 1572872 | tf_op jit(solution)/shard_map/ppermute | solution.py:280
  70.4 0.0 collective-permute-done.1.refs_3_
  70.4 2.0 %collective-permute-start.5 = (bf16[2048,128]{1,0:T(8,128)(2,1)}, bf16[2048,128]{1,0:T(8,128)(2,1)}, u32[]{:S(2)}, u32[]{:S(2)}) collective-permute-start(bf16[2048,128]{1,0:T(8,128)(2,1)} %collective-permute-done.1.refs_3_), channel_id=1, source_target_pairs={{0,64},{64,0},{128,192},{192,128},{256,320},{320,256},{384,448},{4... | collective-permute-start | bytes 1572872 | tf_op jit(solution)/shard_map/ppermute | solution.py:280
  72.4 0.0 collective-permute-done.refs_2_
  72.4 2.3 %collective-permute-start.4 = (bf16[2048,128]{1,0:T(8,128)(2,1)}, bf16[2048,128]{1,0:T(8,128)(2,1)}, u32[]{:S(2)}, u32[]{:S(2)}) collective-permute-start(bf16[2048,128]{1,0:T(8,128)(2,1)} %collective-permute-done.refs_2_), channel_id=1, source_target_pairs={{0,64},{64,0},{128,192},{192,128},{256,320},{320,256},{384,448},{4... | collective-permute-start | bytes 1572872 | tf_op jit(solution)/shard_map/ppermute | solution.py:280
  74.8 3.3 %inside.1 = (f32[256,1024]{1,0:T(8,128)S(1)}, bf16[256,512]{1,0:T(8,128)(2,1)S(1)}, f32[32,256]{1,0:T(8,128)S(1)}) custom-call(f32[256,512]{1,0:T(8,128)S(1)} %get-tuple-element.10.cum_ref, bf16[256,512]{1,0:T(8,128)(2,1)} %bitcast.21, bf16[256,512]{1,0:T(8,128)(2,1)} %bitcast.20, bf16[256,1024]{1,0:T(8,128)(2,1)} %bitcast.17, f32[512,256]{1,0:T(8,128)} %bitcast.18), custom_call_target="tpu_custom_call" | custom-call | flops 300000000 | bytes 1000000 | tf_op jit(solution)/shard_map/inside/pallas_call | solution.py:305
  78.1 0.2 all-to-all-done.got_ref
  78.3 0.2 chain.1
  78.6 18.4 %all_to_all.16 = bf16[16,32,256]{2,1,0:T(8,128)(2,1)S(1)} all-to-all(bf16[16,32,256]{2,1,0:T(8,128)(2,1)S(1)} %chain.1), channel_id=1, replica_groups=mesh['sp'=16,'dp'=64] {'sp'}, dimensions={0} | all-to-all | bytes 524288 | tf_op jit(solution)/shard_map/all_to_all | solution.py:335
  96.9 0.0 collective-permute-done.3.refs_5_
  96.9 0.0 collective-permute-done.6.refs_8_
  96.9 0.0 collective-permute-done.5.refs_7_
  97.0 0.0 collective-permute-done.4.refs_6_
  97.0 3.9 %project.1 = bf16[256,2048]{1,0:T(8,128)(2,1)} custom-call(f32[256,1024]{1,0:T(8,128)S(1)} %get-tuple-element.11.inside_ref, bf16[256,512]{1,0:T(8,128)(2,1)S(1)} %get-tuple-element.12.far_ref, bf16[512,256]{1,0:T(8,128)(2,1)S(1)} %bitcast.10, f32[1,256]{1,0:T(1,128)} %bitcast.23, bf16[2048,128]{1,0:T(8,128)(2,1)} %bitcast.15, ...), custom_call_target="tpu_custom_call" | custom-call | flops 1000000000 | bytes 1000000 | tf_op jit(solution)/shard_map/project/pallas_call | solution.py:337
  (3 shorter events, 0.0 us)
Async XLA Ops:
  43.0 23.0 %copy-start = (bf16[64,32,128]{2,1,0:T(8,128)(2,1)}, bf16[64,32,128]{2,1,0:T(8,128)(2,1)S(1)}, u32[]{:S(2)}) copy-start(bf16[64,32,128]{2,1,0:T(8,128)(2,1)S(1)} %all_to_all.15) | copy-start | bytes 1572868
  43.0 25.1 %collective-permute-start.2 = (bf16[2048,128]{1,0:T(8,128)(2,1)S(1)}, bf16[2048,128]{1,0:T(8,128)(2,1)S(1)}, u32[]{:S(2)}, u32[]{:S(2)}) collective-permute-start(bf16[2048,128]{1,0:T(8,128)(2,1)S(1)} %bitcast.11), channel_id=1, source_target_pairs={{7,0},{0,1},{1,2},{2,3},{3,4},{4,5},{5,6},{6,7},{15,8},{8,9},{9,10... | collective-permute-start | bytes 1572872 | tf_op jit(solution)/shard_map/ppermute | solution.py:277
  46.2 24.2 %collective-permute-start.1 = (bf16[2048,128]{1,0:T(8,128)(2,1)S(1)}, bf16[2048,128]{1,0:T(8,128)(2,1)}, u32[]{:S(2)}, u32[]{:S(2)}) collective-permute-start(bf16[2048,128]{1,0:T(8,128)(2,1)S(1)} %bitcast.12), channel_id=1, source_target_pairs={{8,0},{9,1},{10,2},{11,3},{12,4},{13,5},{14,6},{15,7},{16,8},{17,9... | collective-permute-start | bytes 1572872 | tf_op jit(solution)/shard_map/ppermute | solution.py:277
  48.7 23.7 %collective-permute-start = (bf16[2048,128]{1,0:T(8,128)(2,1)S(1)}, bf16[2048,128]{1,0:T(8,128)(2,1)}, u32[]{:S(2)}, u32[]{:S(2)}) collective-permute-start(bf16[2048,128]{1,0:T(8,128)(2,1)S(1)} %bitcast.13), channel_id=1, source_target_pairs={{1,0},{2,1},{3,2},{4,3},{5,4},{6,5},{7,6},{0,7},{9,8},{10,9},{11,1... | collective-permute-start | bytes 1572872 | tf_op jit(solution)/shard_map/ppermute | solution.py:277
  55.4 22.9 %all-to-all-start = ((bf16[16,72,128]{2,1,0:T(8,128)(2,1)}), bf16[16,72,128]{2,1,0:T(8,128)(2,1)S(1)}, u32[]{:S(2)}, u32[]{:S(2)}) async-start(bf16[16,72,128]{2,1,0:T(8,128)(2,1)} %get-tuple-element.13), calls=%async_computation | async-start | bytes 589824 | tf_op jit(solution)/shard_map/all_to_all | solution.py:303
  66.0 30.9 %collective-permute-start.3 = (bf16[2048,128]{1,0:T(8,128)(2,1)S(1)}, bf16[2048,128]{1,0:T(8,128)(2,1)}, u32[]{:S(2)}, u32[]{:S(2)}) collective-permute-start(bf16[2048,128]{1,0:T(8,128)(2,1)S(1)} %bitcast.14), channel_id=1, source_target_pairs={{0,64},{64,0},{128,192},{192,128},{256,320},{320,256},{384,448},{4... | collective-permute-start | bytes 1572872 | tf_op jit(solution)/shard_map/ppermute | solution.py:280
  68.1 10.0 %copy-start.1 = (bf16[2048,128]{1,0:T(8,128)(2,1)}, bf16[2048,128]{1,0:T(8,128)(2,1)S(1)}, u32[]{:S(2)}) copy-start(bf16[2048,128]{1,0:T(8,128)(2,1)S(1)} %collective-permute-done.2.refs_4_) | copy-start | bytes 1572868
  68.1 28.9 %collective-permute-start.6 = (bf16[2048,128]{1,0:T(8,128)(2,1)S(1)}, bf16[2048,128]{1,0:T(8,128)(2,1)}, u32[]{:S(2)}, u32[]{:S(2)}) collective-permute-start(bf16[2048,128]{1,0:T(8,128)(2,1)S(1)} %collective-permute-done.2.refs_4_), channel_id=1, source_target_pairs={{0,64},{64,0},{128,192},{192,128},{256,320},{320,256},{384,448},{4... | collective-permute-start | bytes 1572872 | tf_op jit(solution)/shard_map/ppermute | solution.py:280
  70.4 26.5 %collective-permute-start.5 = (bf16[2048,128]{1,0:T(8,128)(2,1)}, bf16[2048,128]{1,0:T(8,128)(2,1)}, u32[]{:S(2)}, u32[]{:S(2)}) collective-permute-start(bf16[2048,128]{1,0:T(8,128)(2,1)} %collective-permute-done.1.refs_3_), channel_id=1, source_target_pairs={{0,64},{64,0},{128,192},{192,128},{256,320},{320,256},{384,448},{4... | collective-permute-start | bytes 1572872 | tf_op jit(solution)/shard_map/ppermute | solution.py:280
  72.4 24.5 %collective-permute-start.4 = (bf16[2048,128]{1,0:T(8,128)(2,1)}, bf16[2048,128]{1,0:T(8,128)(2,1)}, u32[]{:S(2)}, u32[]{:S(2)}) collective-permute-start(bf16[2048,128]{1,0:T(8,128)(2,1)} %collective-permute-done.refs_2_), channel_id=1, source_target_pairs={{0,64},{64,0},{128,192},{192,128},{256,320},{320,256},{384,448},{4... | collective-permute-start | bytes 1572872 | tf_op jit(solution)/shard_map/ppermute | solution.py:280
